TPU v7x, 32 devices: a whole 2x2x4 slice. The times are simulated.
32 devices in a mesh: sp: 8 (over z, core), tp: 4 (over y, x).
Axes of the slice: x: 2, y: 2, z: 4, core: 2. Of those that a mesh axis runs over, the one named last changes fastest.
Arguments:
- cell_query_heads: bfloat16 [1024, 2048], P('sp', 'tp'), may hold values from -6 to 6
- cell_key_heads: bfloat16 [1024, 2048], P('sp', 'tp'), may hold values from -6 to 6
- cell_value_heads: bfloat16 [1024, 2048], P('sp', 'tp'), may hold values from -6 to 6
- output_gate_logits: bfloat16 [1024, 2048], P('sp', 'tp'), may hold values from -6 to 6
- input_gate_log: float32 [1024, 16], P('sp', 'tp'), may hold values from -7 to 310
- forget_gate_logits: float32 [1024, 16], P('sp', 'tp'), may hold values from 1 to 14
- extra_log_decay: float32 [1024, 16], P('sp', 'tp'), may hold values from -1 to 0
- documents: int32 [1024], P('sp'), may hold values from 0 to 7, never falling along the last dimension, each value on 1 to 256 neighbouring positions
- head_norm_gain: float32 [2048], P('tp'), may hold values from 0.1 to 1.9
- stream: bfloat16 [1024, 4096], P('sp', 'tp'), may hold values from -6 to 6
- output_weight: bfloat16 [2048, 4096], P(None, 'tp'), may hold values from -0.125 to 0.125
- expert_norm_gain: bfloat16 [4096], P('tp'), may hold values from 0.099609375 to 1.8984375
- expert_choice_index: int32 [1024, 2], P('sp'), may hold values from 0 to 7, all different within a row; in each aligned block of 128 rows (0 to 127, 128 to 255, ...) at most 64 rows name the same one
- routing_weight: float32 [1024, 2], P('sp'), may hold values from 0.2 to 1
- gate_weight: bfloat16 [8, 4096, 2048], P('sp', None, 'tp'), may hold values from -0.09375 to 0.09375
- up_weight: bfloat16 [8, 4096, 2048], P('sp', None, 'tp'), may hold values from -0.09375 to 0.09375
- down_weight: bfloat16 [8, 2048, 4096], P('sp', None, 'tp'), may hold values from -0.125 to 0.125
Outputs:
- output: bfloat16 [1024, 4096], P('sp', 'tp')
Inputs may be any that keep to these rules, and one draw needn't show every extreme that they name: `expert_choice_index`: in the rows of one index of sp no expert is named more than 64 times, a bound that some block reaches. `documents`: never falling; each document 1 to 256 positions, one exactly 256.
All inputs are finite; a program needn't handle non-finite values.
Results may differ from a plain program's by a relative error of at most 0.01.
Values may be sent and summed in bfloat16 or wider, within the bound.
A program may use at most 64 MiB of HBM per device.

v0:
```python
import functools

import jax
import jax.numpy as jnp
from jax import lax
from jax.experimental import pallas as pl
from jax.experimental.pallas import tpu as pltpu
from jax.sharding import PartitionSpec as P

D = 4096
HD = 128
TOPK = 2


EPSILON = 1e-06
LOW_LOG = -1e30
HIGHEST = lax.Precision.HIGHEST


def prefix_2(part, axis, combine, identity):
    place = lax.axis_index(axis)
    gathered = jax.tree.map(lambda a: lax.all_gather(a, axis), part)
    state = jax.tree.map(lambda a, e: jnp.zeros_like(a) + jnp.asarray(e, a.dtype), part, identity)

    def one(turn, state):
        return combine(
            state, jax.tree.map(lambda a: lax.dynamic_index_in_dim(a, turn, 0, False), gathered)
        )

    return lax.fori_loop(0, place, one, state)


def empty_summary(heads, width):
    return (
        jnp.zeros((heads, width, width), jnp.float32),
        jnp.zeros((heads, width), jnp.float32),
        jnp.full((heads,), LOW_LOG, jnp.float32),
        jnp.zeros((heads,), jnp.float32),
        jnp.zeros((), jnp.int32),
        jnp.full((), -1, jnp.int32),
        jnp.full((), -1, jnp.int32),
    )


def block_summary(key_f, value_f, decay_logarithm, input_gate_log, documents, first_global):
    length = documents.shape[0]
    positions = jnp.arange(length, dtype=jnp.int32)
    cumulative = jnp.cumsum(decay_logarithm, axis=0)
    total_log = cumulative[-1]
    prior_log = cumulative - decay_logarithm
    starts = jnp.concatenate([jnp.reshape(first_global, (1,)), documents[1:] != documents[:-1]])
    inside = jnp.any(starts)
    last_start = jnp.max(jnp.where(starts, positions, -1))
    base_log = jnp.sum(jnp.where((positions == last_start)[:, None], prior_log, 0.0), axis=0)
    in_last = (documents == documents[-1])[:, None]
    weight_log = total_log[None, :] - cumulative + input_gate_log
    peak_log = jnp.max(jnp.where(in_last, weight_log, LOW_LOG), axis=0)
    peak_log = jnp.where(inside, jnp.maximum(peak_log, total_log - base_log), peak_log)
    weights = jnp.where(in_last, jnp.exp(jnp.minimum(weight_log - peak_log[None, :], 0.0)), 0.0)
    matrix = jnp.einsum("lhd,lhe->hde", weights[:, :, None] * key_f, value_f, precision=HIGHEST)
    normer = jnp.sum(weights[:, :, None] * key_f, axis=0)
    return (
        matrix,
        normer,
        peak_log,
        total_log,
        inside.astype(jnp.int32),
        documents[0],
        documents[-1],
    )


def combine(early, late):
    broken = late[5] != early[6]
    carry_matrix = jnp.where(broken, 0.0, early[0])
    carry_normer = jnp.where(broken, 0.0, early[1])
    carry_peak = jnp.where(broken, 0.0, early[2])
    joined = jnp.maximum(late[3] + carry_peak, late[2])
    older = jnp.exp(late[3] + carry_peak - joined)
    newer = jnp.exp(late[2] - joined)
    resets = late[4] > 0
    matrix = jnp.where(
        resets, late[0], older[:, None, None] * carry_matrix + newer[:, None, None] * late[0]
    )
    normer = jnp.where(resets, late[1], older[:, None] * carry_normer + newer[:, None] * late[1])
    peak_log = jnp.where(resets, late[2], joined)
    flags = jnp.maximum(jnp.maximum(early[4], late[4]), broken.astype(jnp.int32))
    merged = (matrix, normer, peak_log, early[3] + late[3], flags, early[5], late[6])
    early_empty = early[6] < 0
    late_empty = late[6] < 0
    return tuple(
        (
            jnp.where(early_empty, second, jnp.where(late_empty, first_item, joint))
            for first_item, second, joint in zip(early, late, merged)
        )
    )


def block_output(query_f, key_f, value_f, decay_logarithm, input_gate_log, documents, prefix):
    prev_matrix, prev_normer, prev_peak, _, _, _, prev_last = prefix
    length = documents.shape[0]
    positions = jnp.arange(length, dtype=jnp.int32)
    cumulative = jnp.cumsum(decay_logarithm, axis=0)
    prior_log = cumulative - decay_logarithm
    before = jnp.concatenate([jnp.reshape(prev_last, (1,)), documents[:-1]])
    starts = documents != before
    last_start = lax.cummax(jnp.where(starts, positions, -1), axis=0)
    started = last_start >= 0
    picker = (positions[None, :] == last_start[:, None]).astype(jnp.float32)
    base_log = jnp.dot(picker, prior_log, precision=HIGHEST)
    carry_log = (cumulative + jnp.where(started[:, None], -base_log, prev_peak[None, :])).T
    same_doc = (documents[:, None] == documents[None, :]) & (
        positions[:, None] >= positions[None, :]
    )
    cum_heads = cumulative.T
    pair_log = cum_heads[:, :, None] - cum_heads[:, None, :] + input_gate_log.T[:, None, :]
    pair_log = jnp.where(same_doc[None], pair_log, LOW_LOG)
    peak_log = jnp.maximum(carry_log, jnp.max(pair_log, axis=-1))
    weights = jnp.exp(pair_log - peak_log[:, :, None])
    scores = jnp.einsum("lhd,shd->hls", query_f, key_f, precision=HIGHEST) * weights
    carry_scale = jnp.where(started[None, :], 0.0, jnp.exp(carry_log - peak_log))
    numer = jnp.einsum("hls,she->hle", scores, value_f, precision=HIGHEST)
    numer = numer + carry_scale[:, :, None] * jnp.einsum(
        "lhd,hde->hle", query_f, prev_matrix, precision=HIGHEST
    )
    denom = jnp.sum(scores, axis=-1) + carry_scale * jnp.einsum(
        "lhd,hd->hl", query_f, prev_normer, precision=HIGHEST
    )
    cell_vals = numer / jnp.maximum(jnp.abs(denom), jnp.exp(-peak_log))[:, :, None]
    return jnp.transpose(cell_vals, (1, 0, 2))


def finish_cell(cell_vals, output_gate_logits, head_norm_gain):
    length, heads, width = cell_vals.shape
    gated_cell = (
        jax.nn.sigmoid(output_gate_logits.astype(jnp.float32)).reshape(length, heads, width)
        * cell_vals
    )
    scaled = gated_cell * lax.rsqrt(
        jnp.mean(gated_cell * gated_cell, axis=-1, keepdims=True) + EPSILON
    )
    scaled = scaled * head_norm_gain.reshape(heads, width)
    return scaled.reshape(length, heads * width).astype(jnp.bfloat16)


MESH = pl.DeviceIdType.MESH
PARALLEL_LIMIT = 56 * 1024 * 1024


def remote(src, dst, send, recv, where):
    return pltpu.make_async_remote_copy(src, dst, send, recv, device_id=where, device_id_type=MESH)


def spread_own(teams, j, buf, row, height, width, chunk, send, recv):
    view = buf.at[pl.ds(row, height), pl.ds(pl.multiple_of(j * width, 128), width)]
    copies = []
    if teams == 4:
        for turn, peer in enumerate((j + 1 - 2 * lax.rem(j, 2), lax.rem(j + 2, 4))):
            copies.append(remote(view, view, send.at[chunk, turn], recv.at[chunk, turn], {"tp": peer}))
    else:
        for turn in range(teams - 1):
            peer = lax.rem(j + turn + 1, teams)
            copies.append(remote(view, view, send.at[chunk, turn], recv.at[chunk, turn], {"tp": peer}))
    return copies


def spread_relay(teams, j, buf, row, height, width, chunk, send, recv):
    if teams != 4:
        return []
    half = height // 2
    across, along = j + 1 - 2 * lax.rem(j, 2), lax.rem(j + 2, 4)
    first = buf.at[pl.ds(row, half), pl.ds(pl.multiple_of(across * width, 128), width)]
    second = buf.at[pl.ds(row + half, half), pl.ds(pl.multiple_of(along * width, 128), width)]
    return [
        remote(first, first, send.at[chunk, 2], recv.at[chunk, 2], {"tp": along}),
        remote(second, second, send.at[chunk, 3], recv.at[chunk, 3], {"tp": across}),
    ]


def expert_kernel(
    groups, teams, cap, each, chunks,
    normed, resid, chooser, selectors, weights, gate_hbm, up_hbm, down_hbm,
    out, packed, rows, hidden, result, returned, gate, up, down,
    load_sem, z_send, z_recv, t_send, t_recv, h_send, h_recv, r_send, r_recv,
):
    g, j = lax.axis_index("sp"), lax.axis_index("tp")
    own_chunk = g // each
    tall = each * cap
    width = normed.shape[1]
    hide = gate.shape[1]
    loads = [
        pltpu.make_async_copy(gate_hbm.at[0], gate, load_sem.at[0]),
        pltpu.make_async_copy(up_hbm.at[0], up, load_sem.at[1]),
        pltpu.make_async_copy(down_hbm.at[0], down, load_sem.at[2]),
    ]
    for load in loads:
        load.start()
    barrier = pltpu.get_barrier_semaphore()
    for step in range(1, groups):
        pl.semaphore_signal(
            barrier, inc=1, device_id={"sp": lax.rem(g + step, groups)}, device_id_type=MESH
        )
    if teams == 4:
        peers = (j + 1 - 2 * lax.rem(j, 2), lax.rem(j + 2, 4))
    else:
        peers = tuple(lax.rem(j + step, teams) for step in range(1, teams))
    for peer in peers:
        pl.semaphore_signal(barrier, inc=1, device_id={"tp": peer}, device_id_type=MESH)
    packed[...] = jnp.dot(chooser[...], normed[...], preferred_element_type=jnp.float32).astype(
        jnp.bfloat16
    )
    own = pl.ds(pl.multiple_of(g * cap, cap), cap)
    mine = pl.ds(pl.multiple_of(j * width, 128), width)
    rows[own, mine] = packed[own, :]
    pl.semaphore_wait(barrier, groups - 1 + len(peers))

    def dispatch(target):
        return remote(
            packed.at[pl.ds(pl.multiple_of(target * cap, cap), cap)],
            rows.at[own, mine],
            z_send.at[target],
            z_recv.at[g],
            {"sp": target},
        )

    def give_back(target):
        return remote(
            result.at[pl.ds(pl.multiple_of(target * cap, cap), cap)],
            returned.at[own],
            r_send.at[target],
            r_recv.at[g],
            {"sp": target},
        )

    def over_others(body):
        def one(turn, carry):
            target = lax.rem(own_chunk - turn // each + chunks, chunks) * each + lax.rem(turn, each)

            @pl.when(target != g)
            def _():
                body(target)

            return carry

        lax.fori_loop(0, groups, one, 0)

    over_others(lambda target: dispatch(target).start())

    def stage(i, carry):
        def chunk_of(k):
            return lax.rem(own_chunk + k, chunks)

        @pl.when(i < chunks)
        def _():
            c = chunk_of(i)
            row = pl.multiple_of(c * tall, tall)
            for p in range(each):
                source = c * each + p

                @pl.when(source != g)
                def _():
                    place = rows.at[pl.ds(pl.multiple_of(source * cap, cap), cap), mine]
                    remote(place, place, z_send.at[source], z_recv.at[source], {"sp": source}).wait_recv()

            for copy in spread_own(teams, j, rows, row, tall, width, c, t_send, t_recv):
                copy.start()

        @pl.when((i >= 1) & (i < chunks + 1))
        def _():
            c = chunk_of(i - 1)
            row = pl.multiple_of(c * tall, tall)
            for copy in spread_own(teams, j, rows, row, tall, width, c, t_send, t_recv):
                copy.wait_recv()
            for copy in spread_relay(teams, j, rows, row, tall, width, c, t_send, t_recv):
                copy.start()

        @pl.when((i >= 2) & (i < chunks + 2))
        def _():
            c = chunk_of(i - 2)
            row = pl.multiple_of(c * tall, tall)
            for copy in spread_relay(teams, j, rows, row, tall, width, c, t_send, t_recv):
                copy.wait_recv()

            @pl.when(i == 2)
            def _():
                for load in loads:
                    load.wait()

            block = rows[pl.ds(row, tall), :]
            opened = jnp.dot(block, gate[...], preferred_element_type=jnp.float32)
            raised = jnp.dot(block, up[...], preferred_element_type=jnp.float32)
            made = (opened * jax.nn.sigmoid(opened) * raised).astype(jnp.bfloat16)
            hidden[pl.ds(row, tall), pl.ds(pl.multiple_of(j * hide, 128), hide)] = made
            for copy in spread_own(teams, j, hidden, row, tall, hide, c, h_send, h_recv):
                copy.start()

        @pl.when((i >= 3) & (i < chunks + 3))
        def _():
            c = chunk_of(i - 3)
            row = pl.multiple_of(c * tall, tall)
            for copy in spread_own(teams, j, hidden, row, tall, hide, c, h_send, h_recv):
                copy.wait_recv()
            for copy in spread_relay(teams, j, hidden, row, tall, hide, c, h_send, h_recv):
                copy.start()

        @pl.when(i >= 4)
        def _():
            c = chunk_of(i - 4)
            row = pl.multiple_of(c * tall, tall)
            for copy in spread_relay(teams, j, hidden, row, tall, hide, c, h_send, h_recv):
                copy.wait_recv()
            result[pl.ds(row, tall), :] = jnp.dot(
                hidden[pl.ds(row, tall), :], down[...], preferred_element_type=jnp.float32
            ).astype(jnp.bfloat16)
            for p in range(each):
                target = c * each + p

                @pl.when(target != g)
                def _():
                    give_back(target).start()

                @pl.when(target == g)
                def _():
                    returned[own, :] = result[own, :]

        return carry

    lax.fori_loop(0, chunks + 4, stage, 0)

    def await_back(source):
        place = returned.at[pl.ds(pl.multiple_of(source * cap, cap), cap)]
        remote(place, place, r_send.at[source], r_recv.at[source], {"sp": source}).wait_recv()

    over_others(await_back)
    mixed = resid[...].astype(jnp.float32)
    for ordinal in range(TOPK):
        picked = jnp.dot(selectors[ordinal], returned[...], preferred_element_type=jnp.float32)
        mixed = mixed + weights[:, ordinal : ordinal + 1] * picked
    out[...] = mixed.astype(jnp.bfloat16)

    over_others(lambda target: dispatch(target).wait_send())
    over_others(lambda target: give_back(target).wait_send())

    def drain(c, carry):
        row = pl.multiple_of(c * tall, tall)
        for spread in (spread_own, spread_relay):
            for copy in spread(teams, j, rows, row, tall, width, c, t_send, t_recv):
                copy.wait_send()
            for copy in spread(teams, j, hidden, row, tall, hide, c, h_send, h_recv):
                copy.wait_send()
        return carry

    lax.fori_loop(0, chunks, drain, 0)


def experts(normed, resid, chooser, selectors, weights, gate_weight, up_weight, down_weight, cap):
    groups, teams = lax.axis_size("sp"), lax.axis_size("tp")
    slots = groups * cap
    each = max(1, min(groups, 128 // cap))
    chunks = groups // each
    tokens, width = normed.shape
    _, model, hide = gate_weight.shape
    _, hidden_all, _ = down_weight.shape
    ways = max(4, teams)
    vmem = pl.BlockSpec(memory_space=pltpu.VMEM)
    hbm = pl.BlockSpec(memory_space=pl.ANY)
    bf16 = jnp.bfloat16
    return pl.pallas_call(
        functools.partial(expert_kernel, groups, teams, cap, each, chunks),
        out_shape=jax.ShapeDtypeStruct((tokens, width), bf16),
        in_specs=[vmem] * 5 + [hbm] * 3,
        out_specs=vmem,
        scratch_shapes=[
            pltpu.VMEM((slots, width), bf16),
            pltpu.VMEM((slots, model), bf16),
            pltpu.VMEM((slots, hidden_all), bf16),
            pltpu.VMEM((slots, width), bf16),
            pltpu.VMEM((slots, width), bf16),
            pltpu.VMEM((model, hide), bf16),
            pltpu.VMEM((model, hide), bf16),
            pltpu.VMEM((hidden_all, width), bf16),
            pltpu.SemaphoreType.DMA((3,)),
            pltpu.SemaphoreType.DMA((groups,)),
            pltpu.SemaphoreType.DMA((groups,)),
            pltpu.SemaphoreType.DMA((chunks, ways)),
            pltpu.SemaphoreType.DMA((chunks, ways)),
            pltpu.SemaphoreType.DMA((chunks, ways)),
            pltpu.SemaphoreType.DMA((chunks, ways)),
            pltpu.SemaphoreType.DMA((groups,)),
            pltpu.SemaphoreType.DMA((groups,)),
        ],
        compiler_params=pltpu.CompilerParams(
            collective_id=1, has_side_effects=True, vmem_limit_bytes=PARALLEL_LIMIT
        ),
    )(normed, resid, chooser, selectors, weights, gate_weight, up_weight, down_weight)


def per_device(
    cell_query_heads,
    cell_key_heads,
    cell_value_heads,
    output_gate_logits,
    input_gate_log,
    forget_gate_logits,
    extra_log_decay,
    documents,
    head_norm_gain,
    stream,
    output_weight,
    expert_norm_gain,
    expert_choice_index,
    routing_weight,
    gate_weight,
    up_weight,
    down_weight,
):
    tokens = documents.shape[0]
    local_heads = input_gate_log.shape[1]
    shaped = (tokens, local_heads, HD)
    query_f = cell_query_heads.astype(jnp.float32).reshape(shaped)
    key_f = cell_key_heads.astype(jnp.float32).reshape(shaped) * HD ** (-0.5)
    value_f = cell_value_heads.astype(jnp.float32).reshape(shaped)
    decay_logarithm = jax.nn.log_sigmoid(forget_gate_logits) + extra_log_decay
    first_global = lax.axis_index("sp") == 0
    summary = block_summary(
        key_f, value_f, decay_logarithm, input_gate_log, documents, first_global
    )
    prefix = prefix_2(summary, "sp", combine, empty_summary(local_heads, HD))
    cell_vals = block_output(
        query_f, key_f, value_f, decay_logarithm, input_gate_log, documents, prefix
    )
    memory_cell_output = finish_cell(cell_vals, output_gate_logits, head_norm_gain)
    projected = jnp.dot(
        lax.all_gather(memory_cell_output, "tp", axis=1, tiled=True),
        output_weight,
        preferred_element_type=jnp.float32,
    )
    resid = (stream.astype(jnp.float32) + projected).astype(jnp.bfloat16)
    groups = lax.axis_size("sp")
    experts_all = groups * gate_weight.shape[0]
    capacity = 2 * tokens * TOPK // experts_all
    flat_ids = expert_choice_index.reshape(-1)
    onehot = (flat_ids[:, None] == jnp.arange(experts_all, dtype=jnp.int32)[None, :]).astype(
        jnp.int32
    )
    rank_in = jnp.sum((jnp.cumsum(onehot, axis=0) - onehot) * onehot, axis=1)
    slot_of = (flat_ids * capacity + rank_in).reshape(tokens, TOPK)
    slot_index = jnp.arange(experts_all * capacity, dtype=jnp.int32)
    chooser = jnp.any(slot_index[:, None, None] == slot_of[None, :, :], axis=2).astype(jnp.bfloat16)
    rows_f = resid.astype(jnp.float32)
    squares = lax.psum(jnp.sum(rows_f * rows_f, axis=1), "tp")
    normed = rows_f * lax.rsqrt(squares[:, None] / D + EPSILON)
    normed = (normed * expert_norm_gain.astype(jnp.float32)[None, :]).astype(jnp.bfloat16)
    selectors = (slot_of.T[:, :, None] == slot_index[None, None, :]).astype(jnp.bfloat16)
    return experts(
        normed, resid, chooser, selectors, routing_weight, gate_weight, up_weight, down_weight, capacity
    )


def solution(mesh):
    placed = (
        P("sp", "tp"),
        P("sp", "tp"),
        P("sp", "tp"),
        P("sp", "tp"),
        P("sp", "tp"),
        P("sp", "tp"),
        P("sp", "tp"),
        P("sp"),
        P("tp"),
        P("sp", "tp"),
        P(None, "tp"),
        P("tp"),
        P("sp", None),
        P("sp", None),
        P("sp", None, "tp"),
        P("sp", None, "tp"),
        P("sp", None, "tp"),
    )
    return jax.shard_map(
        per_device, mesh=mesh, in_specs=placed, out_specs=P("sp", "tp"), check_vma=False
    )
```

profile of v0, /device:TPU:9, one launch (start us, length us, event | category | flops | bytes accessed | tf_op | source)
XLA Modules:
  0.0 222.5 jit_solution(13574650342252286373)
XLA Ops:
  6.6 0.7 fusion.31
  7.7 1.5 fusion.38
  9.2 1.2 dynamic-slice
  10.4 2.0 slice_dynamic-update-slice_fusion
  12.5 1.3 broadcast_compare_fusion.1
  13.8 0.7 fusion.35
  14.5 0.6 iota_compare_fusion.7
  15.7 0.9 select_reduce_fusion
  16.6 0.8 select_multiply_fusion
  17.4 1.0 copy.152
  18.4 1.0 copy.158
  19.4 1.1 fusion.20
  20.6 0.7 dynamic-update-slice.1
  21.3 1.4 slice_dynamic-update-slice_fusion.1
  22.7 6.5 %all-reduce.3 = (s32[8]{0:T(128)S(1)}, s32[8]{0:T(128)S(1)}, s32[8]{0:T(128)S(1)}) all-reduce(s32[8]{0:T(128)S(1)} %slice_dynamic-update-slice_fusion.1, s32[8]{0:T(128)S(1)} %dynamic-update-slice.1, s32[8]{0:T(128)S(1)} %get-tuple-element.227), channel_id=1, replica_groups=mesh['sp'=8,'tp'=4] {'sp'}, use_global_device_ids=true, to_apply=%add | all-reduce | flops 24 | bytes 192
  29.2 0.8 copy.139
  30.5 1.0 copy.151
  31.5 1.0 add_divide_fusion
  32.6 0.7 convert_element_type.52
  33.3 0.6 reduce-window.18
  34.5 0.7 convert_element_type.56.chooser
  35.2 0.7 copy.142.weights
  35.9 12.3 %all-gather.2 = f32[8,1,4]{2,1,0:T(1,128)S(1)} all-gather(f32[1,1,4]{2,1,0:T(1,128)S(1)} %bitcast.184), channel_id=1, replica_groups=mesh['sp'=8,'tp'=4] {'sp'}, dimensions={0}, use_global_device_ids=true | all-gather | bytes 144 | tf_op jit(solution)/shard_map/all_gather | solution.py:22
  48.2 9.2 %all-gather.1 = f32[8,1,4]{2,1,0:T(1,128)S(1)} all-gather(f32[1,1,4]{2,1,0:T(1,128)S(1)} %get-tuple-element.222), channel_id=1, replica_groups=mesh['sp'=8,'tp'=4] {'sp'}, dimensions={0}, use_global_device_ids=true | all-gather | bytes 144 | tf_op jit(solution)/shard_map/all_gather | solution.py:22
  57.5 11.3 %all_gather.47 = f32[8,4,128]{2,1,0:T(4,128)S(1)} all-gather(f32[1,4,128]{2,1,0:T(4,128)S(1)} %bitcast.181), channel_id=1, replica_groups=mesh['sp'=8,'tp'=4] {'sp'}, dimensions={0}, use_global_device_ids=true | all-gather | bytes 18432 | tf_op jit(solution)/shard_map/all_gather | solution.py:22
  69.2 0.8 fusion.18.selectors
  70.1 18.7 %while.20 = (s32[]{:T(128)}, f32[4,128,128]{2,1,0:T(8,128)S(1)}, f32[4,128]{1,0:T(4,128)S(1)}, f32[4]{0:T(128)S(1)}, s32[]{:T(128)}, /*index=5*/s32[]{:T(128)}, ...) while((s32[]{:T(128)}, f32[4,128,128]{2,1,0:T(8,128)S(1)}, ...), condition=%wide.region_7.8_spmd, body=%wide.region_6.7_spmd.sunk | while | flops 462383 | bytes 793101 | solution.py:30
  70.1 0.6 dynamic_slice.60
  71.4 0.6 dynamic_slice.62
  72.6 0.6 dynamic_slice.61
  73.8 1.1 bitcast_select_fusion.6
  76.3 0.6 dynamic_slice.60
  77.6 0.6 dynamic_slice.62
  78.8 0.6 dynamic_slice.61
  80.1 1.1 bitcast_select_fusion.6
  82.6 0.6 dynamic_slice.60
  83.8 0.6 dynamic_slice.62
  85.0 0.6 dynamic_slice.61
  86.3 1.1 bitcast_select_fusion.6
  89.5 0.4 fusion.39
  89.8 0.3 convolution_bitcast_fusion.1
  90.4 0.4 multiply_reduce_fusion
  90.9 8.0 %all_gather.48 = bf16[128,2048]{0,1:T(8,128)(2,1)S(1)} all-gather(bf16[128,512]{0,1:T(8,128)(2,1)S(1)} %bitcast.167), channel_id=1, replica_groups=mesh['sp'=8,'tp'=4] {'tp'}, dimensions={1}, use_global_device_ids=true | all-gather | bytes 655360 | tf_op jit(solution)/shard_map/all_gather | solution.py:434
  99.0 3.0 %fusion.14 = (f32[128]{0:T(128)S(1)}, bf16[128,1024]{1,0:T(8,128)(2,1)S(1)}) fusion(bf16[128,2048]{0,1:T(8,128)(2,1)S(1)} %all_gather.48, bf16[2048,1024]{1,0:T(8,128)(2,1)} %param.29, bf16[128,1024]{1,0:T(8,128)(2,1)S(1)} %copy-done.2), kind=kOutput, calls=%fused_computation.35 | convolution fusion | flops 537657216 | bytes 5243392 | tf_op jit(solution)/shard_map/dot_general | solution.py:433
  102.0 6.9 %psum.7 = f32[128]{0:T(128)S(1)} all-reduce(f32[128]{0:T(128)S(1)} %get-tuple-element.235), channel_id=1, replica_groups=mesh['sp'=8,'tp'=4] {'tp'}, use_global_device_ids=true, to_apply=%region_13.14 | all-reduce | flops 128 | bytes 1024 | tf_op jit(solution)/shard_map/psum | solution.py:451
  109.0 0.8 fusion.16.normed
  109.8 104.2 %shard_map.163 = bf16[128,1024]{1,0:T(8,128)(2,1)} custom-call(bf16[128,1024]{1,0:T(8,128)(2,1)} %fusion.16.normed, bf16[128,1024]{1,0:T(8,128)(2,1)} %copy-done, bf16[512,128]{1,0:T(8,128)(2,1)} %convert_element_type.56.chooser, bf16[2,128,512]{2,1,0:T(8,128)(2,1)} %fusion.18.selectors, f32[128,2]{1,0:T(8,128)} %copy.142.weights, ...), custom_call_target="tpu_custom_call" | custom-call | tf_op jit(solution)/shard_map/pallas_call | solution.py:368
  214.0 1.7 copy.188
  (67 shorter events, 3.4 us)
Async XLA Ops:
  6.5 62.3 %copy-start.3 = (s32[128]{0:T(128)S(1)}, s32[128]{0:T(128)}, u32[]{:S(2)}) copy-start(s32[128]{0:T(128)} %param.26) | copy-start | bytes 1540
  6.5 62.4 %copy-start.4 = (f32[128,4]{0,1:T(4,128)S(1)}, f32[128,4]{0,1:T(4,128)}, u32[]{:S(2)}) copy-start(f32[128,4]{0,1:T(4,128)} %param.23) | copy-start | bytes 6148
  6.5 50.9 %copy-start.1 = (bf16[128,512]{1,0:T(8,128)(2,1)S(1)}, bf16[128,512]{1,0:T(8,128)(2,1)}, u32[]{:S(2)}) copy-start(bf16[128,512]{1,0:T(8,128)(2,1)} %param.20) | copy-start | bytes 393220
  6.5 27.9 %copy-start.5 = (s32[128,2]{0,1:T(2,128)S(1)}, s32[128,2]{0,1:T(2,128)}, u32[]{:S(2)}) copy-start(s32[128,2]{0,1:T(2,128)} %param.31) | copy-start | bytes 3076
  6.5 28.7 %copy-start.7 = (f32[128,2]{0,1:T(2,128)S(1)}, f32[128,2]{0,1:T(2,128)}, u32[]{:S(2)}) copy-start(f32[128,2]{0,1:T(2,128)} %param.32) | copy-start | bytes 3076
  6.5 63.5 %all-gather.5.cloned.1.call-start = ((), (), s32[]{:S(2)}) async-start(), calls=%async_computation | async-start | bytes 2359296 | tf_op jit(solution)/shard_map/all_gather | solution.py:22
  69.2 21.6 %copy-start.6 = (f32[512]{0:T(512)S(1)}, f32[512]{0:T(512)}, u32[]{:S(2)}) copy-start(f32[512]{0:T(512)} %param.27) | copy-start | bytes 6148
  70.1 28.9 %copy-start.2 = (bf16[128,1024]{1,0:T(8,128)(2,1)S(1)}, bf16[128,1024]{1,0:T(8,128)(2,1)}, u32[]{:S(2)}) copy-start(bf16[128,1024]{1,0:T(8,128)(2,1)} %param.28) | copy-start | bytes 786436
  102.0 7.8 %copy-start = (bf16[128,1024]{1,0:T(8,128)(2,1)}, bf16[128,1024]{1,0:T(8,128)(2,1)S(1)}, u32[]{:S(2)}) copy-start(bf16[128,1024]{1,0:T(8,128)(2,1)S(1)} %get-tuple-element.236.resid) | copy-start | bytes 786436
Sparse Core Ops, SparseCore 0:
  20.7 30.7 all-gather.4
where the time goes:
time: 224 us; the launch traced here: 223 us
  Pallas kernels  104 us (46%)
  blocking collectives  54.3 us (24%)
  local copies, waits for them, and re-layouts  18.3 us (8%)
  other arithmetic  16 us (7%)
  between operations  14.3 us (6%)
  loops' own time  9.73 us (4%)
  matrix products  5.6 us (2%)
    pallas_call x1, Pallas kernels, experts(): pl.pallas_call(functools.partial(expert_kernel, groups, teams, cap, each,...  104 us
    all_gather x3, blocking collectives, prefix_2(): gathered = jax.tree.map(lambda a: lax.all_gather(a, axis), part)  32.9 us
    another operation x1, loops' own time, prefix_2(): return lax.fori_loop(0, place, one, state)  9.73 us
    unnamed x26, local copies, waits for them, and re-layouts  8.68 us
    all_gather x1, blocking collectives, per_device(): lax.all_gather(memory_cell_output, 'tp', axis=1, tiled=True)  8.03 us
    psum x1, blocking collectives, per_device(): squares = lax.psum(jnp.sum(rows_f * rows_f, axis=1), 'tp')  6.94 us
    unnamed x1, blocking collectives  6.5 us
    dynamic_slice x9, local copies, waits for them, and re-layouts, one(): lax.dynamic_index_in_dim(a, turn, 0, False)  5.34 us
  transfers between devices with their start and end apart: 1, of which 0 were waited for; matrix products, arithmetic and copies ran while one was open for 4% of the time, Pallas kernels for 0%

commit v1 on v0

v1 whole, which is shorter than its diff:
```python
import functools

import jax
import jax.numpy as jnp
from jax import lax
from jax.experimental import pallas as pl
from jax.experimental.pallas import tpu as pltpu
from jax.sharding import PartitionSpec as P

HD = 128
TOPK = 2
EPSILON = 1e-06
LOW_LOG = -1e30
HIGHEST = lax.Precision.HIGHEST
MESH = pl.DeviceIdType.MESH
VMEM_LIMIT = 60 * 1024 * 1024
SUB = 8
EACH = 2
f32, bf16 = jnp.float32, jnp.bfloat16


def remote(src, dst, send, recv, where):
    return pltpu.make_async_remote_copy(src, dst, send, recv, device_id=where, device_id_type=MESH)


def near_peers(teams, j):
    if teams == 4:
        return [j + 1 - 2 * lax.rem(j, 2), lax.rem(j + 2, 4)]
    return [lax.rem(j + step, teams) for step in range(1, teams)]


def all_peers(teams, j):
    if teams == 4:
        return near_peers(teams, j) + [3 - j]
    return near_peers(teams, j)


def spread_own(teams, j, buf, row, height, width, chunk, send, recv):
    view = buf.at[pl.ds(row, height), pl.ds(pl.multiple_of(j * width, 128), width)]
    return [
        remote(view, view, send.at[chunk, turn], recv.at[chunk, turn], {"tp": peer})
        for turn, peer in enumerate(near_peers(teams, j))
    ]


def spread_relay(teams, j, buf, row, height, width, chunk, send, recv):
    if teams != 4:
        return []
    half = height // 2
    across, along = near_peers(teams, j)
    first = buf.at[pl.ds(row, half), pl.ds(pl.multiple_of(across * width, 128), width)]
    second = buf.at[pl.ds(row + half, half), pl.ds(pl.multiple_of(along * width, 128), width)]
    return [
        remote(first, first, send.at[chunk, 2], recv.at[chunk, 2], {"tp": along}),
        remote(second, second, send.at[chunk, 3], recv.at[chunk, 3], {"tp": across}),
    ]


def nt(a, b, precision=None):
    return lax.dot_general(
        a, b, (((1,), (1,)), ((), ())), precision=precision, preferred_element_type=f32
    )


def kernel(
    groups, teams, heads, reach, cap, each, chunks,
    query, key, value, gate_out, table, head_gain, stream, row_gain, wo_hbm, gate_hbm, up_hbm, down_hbm,
    out,
    kbuf, vbuf, tbuf, cell, ssq, chooser, comb, resid, normed, packed, rows, hidden, result, returned,
    wo, gate, up, down,
    load_sem, k_send, k_recv, v_send, v_recv, m_send, m_recv, c_send, c_recv, s_send, s_recv,
    z_send, z_recv, t_send, t_recv, h_send, h_recv, r_send, r_recv,
):
    g, j = lax.axis_index("sp"), lax.axis_index("tp")
    tokens, width = stream.shape
    hide = gate.shape[1]
    span = heads * HD
    slots = groups * cap
    tall = each * cap
    model = width * teams
    loads = [
        pltpu.make_async_copy(wo_hbm, wo, load_sem.at[0]),
        pltpu.make_async_copy(gate_hbm.at[0], gate, load_sem.at[1]),
        pltpu.make_async_copy(up_hbm.at[0], up, load_sem.at[2]),
        pltpu.make_async_copy(down_hbm.at[0], down, load_sem.at[3]),
    ]
    for load in loads:
        load.start()
    barrier = pltpu.get_barrier_semaphore()
    for step in range(1, groups):
        pl.semaphore_signal(
            barrier, inc=1, device_id={"sp": lax.rem(g + step, groups)}, device_id_type=MESH
        )
    peers = all_peers(teams, j)
    for peer in peers:
        pl.semaphore_signal(barrier, inc=1, device_id={"tp": peer}, device_id_type=MESH)
    pl.semaphore_wait(barrier, groups - 1 + len(peers))

    def send_table(r):
        return remote(table, tbuf.at[r - 1], m_send.at[r - 1], m_recv.at[r - 1], {"sp": g + r})

    def send_pair(r, h):
        cols = pl.ds(h * HD, HD)
        return [
            remote(key.at[:, cols], kbuf.at[r - 1, :, cols], k_send.at[r - 1, h], k_recv.at[r - 1, h], {"sp": g + r}),
            remote(value.at[:, cols], vbuf.at[r - 1, :, cols], v_send.at[r - 1, h], v_recv.at[r - 1, h], {"sp": g + r}),
        ]

    for r in range(1, reach + 1):

        @pl.when(g + r < groups)
        def _(r=r):
            send_table(r).start()

    for h in range(heads):
        for r in range(1, reach + 1):

            @pl.when(g + r < groups)
            def _(r=r, h=h):
                for copy in send_pair(r, h):
                    copy.start()

    for r in range(1, reach + 1):

        @pl.when(g < r)
        def _(r=r):
            kbuf[r - 1] = jnp.zeros_like(kbuf[r - 1])
            vbuf[r - 1] = jnp.zeros_like(vbuf[r - 1])
            tbuf[r - 1] = jnp.full(tbuf.shape[1:], -1.0, f32)

    down_iota = lax.broadcasted_iota(jnp.int32, (tokens, tokens), 0)
    across_iota = lax.broadcasted_iota(jnp.int32, (tokens, tokens), 1)
    causal = across_iota <= down_iota
    lower = causal.astype(f32)
    upper = (down_iota <= across_iota).astype(f32)
    strict = (down_iota < across_iota).astype(bf16)
    eye = (down_iota == across_iota).astype(f32)
    misc = table[2 * SUB : 3 * SUB, :]
    columns = nt(eye, misc, HIGHEST)
    expert_pad = -(-groups // SUB) * SUB
    expert_iota = lax.broadcasted_iota(jnp.int32, (expert_pad, tokens), 0).astype(f32)
    member = jnp.zeros((expert_pad, tokens), f32)
    weighted = jnp.zeros((expert_pad, tokens), f32)
    for ordinal in range(TOPK):
        chosen = expert_iota == misc[1 + ordinal : 2 + ordinal, :]
        member = member + jnp.where(chosen, 1.0, 0.0)
        weighted = weighted + jnp.where(
            chosen, misc[1 + TOPK + ordinal : 2 + TOPK + ordinal, :], 0.0
        )
    rank = jnp.dot(member.astype(bf16), strict, preferred_element_type=f32)
    rank = jnp.where(member > 0.5, rank, -1.0)
    cap_iota = lax.broadcasted_iota(jnp.int32, (cap, tokens), 0).astype(f32)
    for e in range(groups):
        chooser[e * cap : (e + 1) * cap, :] = jnp.where(
            cap_iota == rank[e : e + 1, :], 1.0, 0.0
        ).astype(bf16)
    slot_line = lax.broadcasted_iota(jnp.int32, (1, slots), 1).astype(f32)
    expert_line = jnp.floor((slot_line + 0.5) * (1.0 / cap))
    place_line = slot_line - expert_line * cap
    expand = (
        lax.broadcasted_iota(jnp.int32, (expert_pad, slots), 0).astype(f32) == expert_line
    ).astype(f32)
    rank_wide = jnp.dot(nt(eye, rank), expand, preferred_element_type=f32)
    weight_wide = jnp.dot(
        nt(eye, weighted, HIGHEST), expand, precision=HIGHEST, preferred_element_type=f32
    )
    comb[...] = jnp.where(rank_wide == place_line, weight_wide, 0.0).astype(bf16)

    decay = table[0:SUB, :]
    entry = table[SUB : 2 * SUB, :]
    doc_col = columns[:, 0:1]
    own_mask = causal & (doc_col == misc[0:1, :])
    cum_col = nt(lower, decay, HIGHEST)
    cum_row = jnp.dot(decay, upper, precision=HIGHEST, preferred_element_type=f32)
    carry = nt(own_mask.astype(f32), decay, HIGHEST)
    masks, terms = [own_mask], [entry - cum_row]

    for r in range(1, reach + 1):

        @pl.when(g >= r)
        def _(r=r):
            send_table(r).wait_recv()

    behind = jnp.zeros((SUB, 1), f32)
    for r in range(1, reach + 1):
        decay_r = tbuf[r - 1, 0:SUB, :]
        mask_r = doc_col == tbuf[r - 1, 2 * SUB : 2 * SUB + 1, :]
        cum_r = jnp.dot(decay_r, upper, precision=HIGHEST, preferred_element_type=f32)
        total_r = cum_r[:, tokens - 1 : tokens]
        terms.append(tbuf[r - 1, SUB : 2 * SUB, :] + ((total_r - cum_r) + behind))
        behind = behind + total_r
        carry = carry + nt(mask_r.astype(f32), decay_r, HIGHEST)
        masks.append(mask_r)

    def cell_copies(h):
        view = cell.at[:, pl.ds(pl.multiple_of(j * span + h * HD, 128), HD)]
        return [
            remote(view, view, c_send.at[h, turn], c_recv.at[h, turn], {"tp": peer})
            for turn, peer in enumerate(peers)
        ]

    for h in range(heads):
        cols = slice(h * HD, (h + 1) * HD)
        for r in range(1, reach + 1):

            @pl.when(g >= r)
            def _(r=r, h=h):
                for copy in send_pair(r, h):
                    copy.wait_recv()

        q_h = query[:, cols]
        keys = [key[:, cols]] + [kbuf[r, :, cols] for r in range(reach)]
        values = [value[:, cols]] + [vbuf[r, :, cols] for r in range(reach)]
        peak = carry[:, h : h + 1]
        logs = []
        for mask, term in zip(masks, terms):
            log = jnp.where(mask, cum_col[:, h : h + 1] + term[h : h + 1, :], LOW_LOG)
            peak = jnp.maximum(peak, jnp.max(log, axis=1, keepdims=True))
            logs.append(log)
        denom = jnp.zeros((tokens, 1), f32)
        numer = jnp.zeros((tokens, HD), f32)
        for log, k_b, v_b in zip(logs, keys, values):
            score = nt(q_h, k_b) * (HD ** -0.5) * jnp.exp(log - peak)
            denom = denom + jnp.sum(score, axis=1, keepdims=True)
            numer = numer + jnp.dot(score.astype(bf16), v_b, preferred_element_type=f32)
        value_h = numer / jnp.maximum(jnp.abs(denom), jnp.exp(-peak))
        value_h = value_h * jax.nn.sigmoid(gate_out[:, cols].astype(f32))
        square = jnp.sum(value_h * value_h, axis=1, keepdims=True) * (1.0 / HD)
        value_h = value_h * lax.rsqrt(square + EPSILON) * head_gain[:, cols]
        cell[:, pl.ds(pl.multiple_of(j * span + h * HD, 128), HD)] = value_h.astype(bf16)
        for copy in cell_copies(h):
            copy.start()

    loads[0].wait()
    half = max(1, heads // 2)
    projected = stream[...].astype(f32)
    for first in range(0, heads, half):
        for h in range(first, first + half):
            for copy in cell_copies(h):
                copy.wait_recv()
        for p in range(teams):
            piece = slice(p * span + first * HD, p * span + (first + half) * HD)
            projected = projected + jnp.dot(cell[:, piece], wo[piece, :], preferred_element_type=f32)
    resid[...] = projected.astype(bf16)
    rows_f = resid[...].astype(f32)
    squares = jnp.sum(rows_f * rows_f, axis=1, keepdims=True)
    ssq[j] = jnp.broadcast_to(squares, (tokens, tokens)).T[0:SUB, :]

    def square_copies():
        return [
            remote(ssq.at[j], ssq.at[j], s_send.at[turn], s_recv.at[turn], {"tp": peer})
            for turn, peer in enumerate(peers)
        ]

    for copy in square_copies():
        copy.start()
    for copy in square_copies():
        copy.wait_recv()
    total = ssq[0]
    for p in range(1, teams):
        total = total + ssq[p]
    total = jnp.broadcast_to(total[0:1, :], (tokens, tokens)).T[:, 0:1]
    scale = lax.rsqrt(total * (1.0 / model) + EPSILON)
    normed[...] = (rows_f * scale * row_gain[...].astype(f32)).astype(bf16)

    own = pl.ds(pl.multiple_of(g * cap, cap), cap)
    mine = pl.ds(pl.multiple_of(j * width, 128), width)
    block = g // each

    def chunk_of(k):
        if chunks == 4:
            pair = block + 1 - 2 * lax.rem(block, 2)
            return jnp.where(
                k == 0, block, jnp.where(k == 1, lax.rem(block + 2, 4), jnp.where(k == 2, 3 - block, pair))
            )
        return lax.rem(block + k, chunks)

    def slot_rows(e):
        return pl.ds(pl.multiple_of(e * cap, cap), cap)

    def dispatch(target):
        return remote(
            packed.at[slot_rows(target)], rows.at[own, mine], z_send.at[target], z_recv.at[g], {"sp": target}
        )

    def give_back(target):
        return remote(
            result.at[slot_rows(target)], returned.at[own], r_send.at[target], r_recv.at[g], {"sp": target}
        )

    def over_others(body):
        def one(k, carry_):
            c = chunk_of(k)
            for p in range(each):
                target = c * each + p

                @pl.when(target != g)
                def _():
                    body(target)

            return carry_

        lax.fori_loop(0, chunks, one, 0)

    def pack(k, carry_):
        c = chunk_of(k)
        at = pl.ds(pl.multiple_of(c * tall, tall), tall)
        packed[at, :] = jnp.dot(chooser[at, :], normed[...], preferred_element_type=f32).astype(bf16)

        @pl.when(k == 0)
        def _():
            rows[own, mine] = packed[own, :]

        for p in range(each):
            target = c * each + p

            @pl.when(target != g)
            def _():
                dispatch(target).start()

        return carry_

    lax.fori_loop(0, chunks, pack, 0)

    def row_of(c):
        return pl.multiple_of(c * tall, tall)

    def start_spread(c):
        for p in range(each):
            source = c * each + p

            @pl.when(source != g)
            def _():
                place = rows.at[slot_rows(source), mine]
                remote(place, place, z_send.at[source], z_recv.at[source], {"sp": source}).wait_recv()

        for copy in spread_own(teams, j, rows, row_of(c), tall, width, c, t_send, t_recv):
            copy.start()

    def finish(c):
        row = row_of(c)
        for copy in spread_relay(teams, j, hidden, row, tall, hide, c, h_send, h_recv):
            copy.wait_recv()
        result[pl.ds(row, tall), :] = jnp.dot(
            hidden[pl.ds(row, tall), :], down[...], preferred_element_type=f32
        ).astype(bf16)
        for p in range(each):
            target = c * each + p

            @pl.when(target != g)
            def _():
                give_back(target).start()

            @pl.when(target == g)
            def _():
                returned[own, :] = result[own, :]

    def hidden_relay(c):
        row = row_of(c)
        for copy in spread_own(teams, j, hidden, row, tall, hide, c, h_send, h_recv):
            copy.wait_recv()
        for copy in spread_relay(teams, j, hidden, row, tall, hide, c, h_send, h_recv):
            copy.start()

    start_spread(chunk_of(0))
    for load in loads[1:]:
        load.wait()

    def stage(k, carry_):
        c = chunk_of(k)
        last = chunk_of(jnp.maximum(k - 1, 0))
        row = row_of(c)

        @pl.when(k < chunks)
        def _():
            for copy in spread_own(teams, j, rows, row, tall, width, c, t_send, t_recv):
                copy.wait_recv()
            for copy in spread_relay(teams, j, rows, row, tall, width, c, t_send, t_recv):
                copy.start()

        @pl.when(k < chunks - 1)
        def _():
            start_spread(chunk_of(k + 1))

        @pl.when(k >= 1)
        def _():
            hidden_relay(last)

        @pl.when(k < chunks)
        def _():
            for copy in spread_relay(teams, j, rows, row, tall, width, c, t_send, t_recv):
                copy.wait_recv()
            block_rows = rows[pl.ds(row, tall), :]
            opened = jnp.dot(block_rows, gate[...], preferred_element_type=f32)
            raised = jnp.dot(block_rows, up[...], preferred_element_type=f32)
            made = (opened * jax.nn.sigmoid(opened) * raised).astype(bf16)
            hidden[pl.ds(row, tall), pl.ds(pl.multiple_of(j * hide, 128), hide)] = made
            for copy in spread_own(teams, j, hidden, row, tall, hide, c, h_send, h_recv):
                copy.start()

        @pl.when(k >= 1)
        def _():
            finish(last)

        return carry_

    lax.fori_loop(0, chunks + 1, stage, 0)

    def await_back(source):
        place = returned.at[slot_rows(source)]
        remote(place, place, r_send.at[source], r_recv.at[source], {"sp": source}).wait_recv()

    over_others(await_back)
    mixed = jnp.dot(comb[...], returned[...], preferred_element_type=f32)
    out[...] = (resid[...].astype(f32) + mixed).astype(bf16)

    for r in range(1, reach + 1):

        @pl.when(g + r < groups)
        def _(r=r):
            send_table(r).wait_send()
            for h in range(heads):
                for copy in send_pair(r, h):
                    copy.wait_send()

    for h in range(heads):
        for copy in cell_copies(h):
            copy.wait_send()
    for copy in square_copies():
        copy.wait_send()
    over_others(lambda target: dispatch(target).wait_send())
    over_others(lambda target: give_back(target).wait_send())

    def drain(c, carry_):
        row = row_of(c)
        for spread in (spread_own, spread_relay):
            for copy in spread(teams, j, rows, row, tall, width, c, t_send, t_recv):
                copy.wait_send()
            for copy in spread(teams, j, hidden, row, tall, hide, c, h_send, h_recv):
                copy.wait_send()
        return carry_

    lax.fori_loop(0, chunks, drain, 0)


def padded(a):
    return jnp.pad(a, ((0, SUB - a.shape[0]), (0, 0)))


def per_device(
    cell_query_heads,
    cell_key_heads,
    cell_value_heads,
    output_gate_logits,
    input_gate_log,
    forget_gate_logits,
    extra_log_decay,
    documents,
    head_norm_gain,
    stream,
    output_weight,
    expert_norm_gain,
    expert_choice_index,
    routing_weight,
    gate_weight,
    up_weight,
    down_weight,
):
    groups, teams = lax.axis_size("sp"), lax.axis_size("tp")
    tokens, heads = input_gate_log.shape
    span = heads * HD
    width = stream.shape[1]
    _, model, hide = gate_weight.shape
    _, hidden_all, _ = down_weight.shape
    experts_all = groups * gate_weight.shape[0]
    cap = 2 * tokens * TOPK // experts_all
    slots = groups * cap
    each = max(1, min(groups, EACH * 64 // cap))
    chunks = groups // each
    reach = max(1, groups // 4)
    ways = max(4, teams)
    others = teams - 1
    decay = jax.nn.log_sigmoid(forget_gate_logits) + extra_log_decay
    misc = jnp.concatenate(
        [documents.astype(f32)[None, :], expert_choice_index.astype(f32).T, routing_weight.T], axis=0
    )
    table = jnp.concatenate([padded(decay.T), padded(input_gate_log.T), padded(misc)], axis=0)
    vmem = pl.BlockSpec(memory_space=pltpu.VMEM)
    hbm = pl.BlockSpec(memory_space=pl.ANY)
    dma = pltpu.SemaphoreType.DMA
    return pl.pallas_call(
        functools.partial(kernel, groups, teams, heads, reach, cap, each, chunks),
        out_shape=jax.ShapeDtypeStruct((tokens, width), bf16),
        in_specs=[vmem] * 8 + [hbm] * 4,
        out_specs=vmem,
        scratch_shapes=[
            pltpu.VMEM((reach, tokens, span), bf16),
            pltpu.VMEM((reach, tokens, span), bf16),
            pltpu.VMEM((reach, 3 * SUB, tokens), f32),
            pltpu.VMEM((tokens, teams * span), bf16),
            pltpu.VMEM((teams, SUB, tokens), f32),
            pltpu.VMEM((slots, tokens), bf16),
            pltpu.VMEM((tokens, slots), bf16),
            pltpu.VMEM((tokens, width), bf16),
            pltpu.VMEM((tokens, width), bf16),
            pltpu.VMEM((slots, width), bf16),
            pltpu.VMEM((slots, model), bf16),
            pltpu.VMEM((slots, hidden_all), bf16),
            pltpu.VMEM((slots, width), bf16),
            pltpu.VMEM((slots, width), bf16),
            pltpu.VMEM(output_weight.shape, bf16),
            pltpu.VMEM((model, hide), bf16),
            pltpu.VMEM((model, hide), bf16),
            pltpu.VMEM((hidden_all, width), bf16),
            dma((4,)),
            dma((reach, heads)),
            dma((reach, heads)),
            dma((reach, heads)),
            dma((reach, heads)),
            dma((reach,)),
            dma((reach,)),
            dma((heads, others)),
            dma((heads, others)),
            dma((others,)),
            dma((others,)),
            dma((groups,)),
            dma((groups,)),
            dma((chunks, ways)),
            dma((chunks, ways)),
            dma((chunks, ways)),
            dma((chunks, ways)),
            dma((groups,)),
            dma((groups,)),
        ],
        compiler_params=pltpu.CompilerParams(
            collective_id=1, has_side_effects=True, vmem_limit_bytes=VMEM_LIMIT
        ),
    )(
        cell_query_heads,
        cell_key_heads,
        cell_value_heads,
        output_gate_logits,
        table,
        head_norm_gain[None, :],
        stream,
        expert_norm_gain[None, :],
        output_weight,
        gate_weight,
        up_weight,
        down_weight,
    )


def solution(mesh):
    placed = (
        P("sp", "tp"),
        P("sp", "tp"),
        P("sp", "tp"),
        P("sp", "tp"),
        P("sp", "tp"),
        P("sp", "tp"),
        P("sp", "tp"),
        P("sp"),
        P("tp"),
        P("sp", "tp"),
        P(None, "tp"),
        P("tp"),
        P("sp", None),
        P("sp", None),
        P("sp", None, "tp"),
        P("sp", None, "tp"),
        P("sp", None, "tp"),
    )
    return jax.shard_map(
        per_device, mesh=mesh, in_specs=placed, out_specs=P("sp", "tp"), check_vma=False
    )
```

time: 224 us -> 105 us (0.47)
  blocking collectives: 54.3 us -> 0 us
  local copies, waits for them, and re-layouts: 18.3 us -> 2.94 us
  between operations: 14.3 us -> 0.01 us
  other arithmetic: 16 us -> 4.03 us
  loops' own time: 9.73 us -> 0 us
  Pallas kernels: 104 us -> 97.2 us
  matrix products: 5.6 us -> 0 us
    all_gather x4 -> x0, blocking collectives: 40.9 us -> none  [the longest x3 32.9 us: prefix_2(): gathered = jax.tree.map(lambda a: lax.all_gather(a, axis), part)]
    another operation x1 -> x0, loops' own time: 9.73 us -> none  [prefix_2(): return lax.fori_loop(0, place, one, state)]
    unnamed x26 -> x1, local copies, waits for them, and re-layouts: 8.68 us -> 1.67 us
    psum x1 -> x0, blocking collectives: 6.94 us -> none  [per_device(): squares = lax.psum(jnp.sum(rows_f * rows_f, axis=1), 'tp')]
    pallas_call x1, Pallas kernels: 104 us -> 97.2 us  [per_device(): pl.pallas_call(functools.partial(kernel, groups, teams, heads, reach, cap...]
    unnamed x1 -> x0, blocking collectives: 6.5 us -> none
    dot_general x7 -> x0, matrix products: 5.6 us -> none  [the longest x1 3.04 us: per_device(): jnp.dot(lax.all_gather(memory_cell_output, 'tp', axis=1, tiled=True), out...]
    dynamic_slice x9 -> x0, local copies, waits for them, and re-layouts: 5.34 us -> none  [one(): lax.dynamic_index_in_dim(a, turn, 0, False)]
  transfers between devices with their start and end apart: 1 -> 0, of which waited for: 0 -> 0; matrix products, arithmetic and copies ran while one was open for 4% -> 0% of each run, Pallas kernels for 0% -> 0%
where the time goes in v1:
time: 105 us; the launch traced here: 104 us
  Pallas kernels  97.2 us (93%)
  other arithmetic  4.03 us (4%)
  local copies, waits for them, and re-layouts  2.94 us (3%)
    pallas_call x1, Pallas kernels, per_device(): pl.pallas_call(functools.partial(kernel, groups, teams, heads, reach, cap...  97.2 us

profile of v1, /device:TPU:9, one launch (start us, length us, event | category | flops | bytes accessed | tf_op | source)
XLA Modules:
  0.0 104.2 jit_solution(2111580199498300775)
XLA Ops:
  0.0 0.7 convert_bitcast_fusion.1
  0.7 0.7 convert_bitcast_fusion
  1.3 0.7 fusion.4
  2.1 0.7 select_maximum_fusion.1
  2.7 1.3 %broadcast_in_dim.11.row_gain = bf16[1,1024]{1,0:T(2,128)(2,1)} reshape(bf16[1024]{0:T(1024)(128)(2,1)} %param.28) | data formatting | bytes 4096 | tf_op jit(solution)/shard_map/broadcast_in_dim | solution.py:546
  4.0 1.3 %fusion.table = f32[24,128]{1,0:T(8,128)} fusion(f32[4,128]{1,0:T(4,128)} %bitcast.9, f32[4,128]{1,0:T(4,128)S(1)} %fusion.4, f32[8,128]{1,0:T(8,128)S(1)} %select_maximum_fusion.1), kind=kLoop, calls=%fused_computation.3 | loop fusion | flops 24576 | bytes 20480 | tf_op jit(solution)/shard_map/concatenate | solution.py:487
  5.3 97.2 %shard_map.163 = bf16[128,1024]{1,0:T(8,128)(2,1)} custom-call(bf16[128,512]{1,0:T(8,128)(2,1)} %query.1, bf16[128,512]{1,0:T(8,128)(2,1)} %key.1, bf16[128,512]{1,0:T(8,128)(2,1)} %value.1, bf16[128,512]{1,0:T(8,128)(2,1)} %gate_out.1, f32[24,128]{1,0:T(8,128)} %fusion.table, f32[1,512]{1,0:T(1,128)} %bitcast.10, bf16[128,1024]{1,0:T(8,128)(2,1)} %stream.1, ...), custom_call_target="tpu_custom_call" | custom-call | tf_op jit(solution)/shard_map/pallas_call | solution.py:491
  102.6 1.7 %copy.19 = bf16[128,1024]{1,0:T(8,128)(2,1)} copy(bf16[128,1024]{1,0:T(8,128)(2,1)} %shard_map.163) | data formatting | bytes 524288

commit v2 on v1

--- a/solution.py
+++ b/solution.py
@@ -15,7 +15,8 @@
 MESH = pl.DeviceIdType.MESH
 VMEM_LIMIT = 60 * 1024 * 1024
 SUB = 8
-EACH = 2
+EACH = 1
+ORDER = ((0, 0), (1, 0), (2, 0), (2, 1), (3, 0), (3, 1), (1, 1), (0, 1))
 f32, bf16 = jnp.float32, jnp.bfloat16
 
 
@@ -64,13 +65,20 @@
 
 def kernel(
     groups, teams, heads, reach, cap, each, chunks,
-    query, key, value, gate_out, table, head_gain, stream, row_gain, wo_hbm, gate_hbm, up_hbm, down_hbm,
-    out,
-    kbuf, vbuf, tbuf, cell, ssq, chooser, comb, resid, normed, packed, rows, hidden, result, returned,
-    wo, gate, up, down,
-    load_sem, k_send, k_recv, v_send, v_recv, m_send, m_recv, c_send, c_recv, s_send, s_recv,
-    z_send, z_recv, t_send, t_recv, h_send, h_recv, r_send, r_recv,
+    *refs,
 ):
+    inputs, (out, *refs) = refs[:17], refs[17:]
+    locals_, refs = refs[:17], refs[17:]
+    (
+        key, value, forget_t, entry_t, extra_t, docs, choice_t, weight_t, query, gate_out, head_gain, stream, row_gain,
+        wo, gate, up, down,
+    ) = locals_
+    (
+        table, kbuf, vbuf, tbuf, cell, ssq, scales, scales_in, chooser, comb, resid, normed, packed, rows, hidden,
+        result, returned,
+        load_sem, k_send, k_recv, v_send, v_recv, f_send, m_send, m_recv, c_send, c_recv, s_send, s_recv,
+        n_send, n_recv, z_send, z_recv, t_send, t_recv, h_send, h_recv, r_send, r_recv,
+    ) = refs
     g, j = lax.axis_index("sp"), lax.axis_index("tp")
     tokens, width = stream.shape
     hide = gate.shape[1]
@@ -79,10 +87,10 @@
     tall = each * cap
     model = width * teams
     loads = [
-        pltpu.make_async_copy(wo_hbm, wo, load_sem.at[0]),
-        pltpu.make_async_copy(gate_hbm.at[0], gate, load_sem.at[1]),
-        pltpu.make_async_copy(up_hbm.at[0], up, load_sem.at[2]),
-        pltpu.make_async_copy(down_hbm.at[0], down, load_sem.at[3]),
+        pltpu.make_async_copy(
+            there.at[0] if len(there.shape) > len(here.shape) else there, here, load_sem.at[i]
+        )
+        for i, (there, here) in enumerate(zip(inputs, locals_))
     ]
     for load in loads:
         load.start()
@@ -94,6 +102,17 @@
     peers = all_peers(teams, j)
     for peer in peers:
         pl.semaphore_signal(barrier, inc=1, device_id={"tp": peer}, device_id_type=MESH)
+    table[...] = jnp.zeros_like(table)
+    for load in loads[:8]:
+        load.wait()
+    forget = forget_t[...]
+    table[0:heads, :] = (
+        jnp.minimum(forget, 0.0) - jnp.log1p(jnp.exp(-jnp.abs(forget))) + extra_t[...]
+    )
+    table[SUB : SUB + heads, :] = entry_t[...]
+    table[2 * SUB : 2 * SUB + 1, :] = docs[...].astype(f32)
+    table[2 * SUB + 1 : 2 * SUB + 1 + TOPK, :] = choice_t[...].astype(f32)
+    table[2 * SUB + 1 + TOPK : 2 * SUB + 1 + 2 * TOPK, :] = weight_t[...]
     pl.semaphore_wait(barrier, groups - 1 + len(peers))
 
     def send_table(r):
@@ -112,10 +131,24 @@
         def _(r=r):
             send_table(r).start()
 
+    shared = groups == 8
+
+    def sends(r):
+        return (g + r < groups) & (lax.rem(g, 2) == 0) if shared and r == 2 else g + r < groups
+
+    hands_on = (lax.rem(g, 2) == 0) & (g >= 2)
+
+    def hand_on(h):
+        cols = pl.ds(h * HD, HD)
+        return [
+            remote(kbuf.at[0, :, cols], kbuf.at[1, :, cols], f_send.at[0, h], k_recv.at[1, h], {"sp": g + 1}),
+            remote(vbuf.at[0, :, cols], vbuf.at[1, :, cols], f_send.at[1, h], v_recv.at[1, h], {"sp": g + 1}),
+        ]
+
     for h in range(heads):
         for r in range(1, reach + 1):
 
-            @pl.when(g + r < groups)
+            @pl.when(sends(r))
             def _(r=r, h=h):
                 for copy in send_pair(r, h):
                     copy.start()
@@ -192,6 +225,9 @@
         carry = carry + nt(mask_r.astype(f32), decay_r, HIGHEST)
         masks.append(mask_r)
 
+    for load in loads[8:13]:
+        load.wait()
+
     def cell_copies(h):
         view = cell.at[:, pl.ds(pl.multiple_of(j * span + h * HD, 128), HD)]
         return [
@@ -207,6 +243,13 @@
             def _(r=r, h=h):
                 for copy in send_pair(r, h):
                     copy.wait_recv()
+
+            if shared and r == 1:
+
+                @pl.when(hands_on)
+                def _(h=h):
+                    for copy in hand_on(h):
+                        copy.start()
 
         q_h = query[:, cols]
         keys = [key[:, cols]] + [kbuf[r, :, cols] for r in range(reach)]
@@ -231,7 +274,7 @@
         for copy in cell_copies(h):
             copy.start()
 
-    loads[0].wait()
+    loads[13].wait()
     half = max(1, heads // 2)
     projected = stream[...].astype(f32)
     for first in range(0, heads, half):
@@ -254,26 +297,27 @@
 
     for copy in square_copies():
         copy.start()
-    for copy in square_copies():
-        copy.wait_recv()
-    total = ssq[0]
-    for p in range(1, teams):
-        total = total + ssq[p]
-    total = jnp.broadcast_to(total[0:1, :], (tokens, tokens)).T[:, 0:1]
-    scale = lax.rsqrt(total * (1.0 / model) + EPSILON)
-    normed[...] = (rows_f * scale * row_gain[...].astype(f32)).astype(bf16)
-
+    normed[...] = (rows_f * row_gain[...].astype(f32).reshape(1, width)).astype(bf16)
     own = pl.ds(pl.multiple_of(g * cap, cap), cap)
     mine = pl.ds(pl.multiple_of(j * width, 128), width)
     block = g // each
 
     def chunk_of(k):
-        if chunks == 4:
-            pair = block + 1 - 2 * lax.rem(block, 2)
-            return jnp.where(
-                k == 0, block, jnp.where(k == 1, lax.rem(block + 2, 4), jnp.where(k == 2, 3 - block, pair))
-            )
-        return lax.rem(block + k, chunks)
+        if groups != 8:
+            return lax.rem(block + k, chunks)
+        chip, side = g // 2, lax.rem(g, 2)
+        steps = [(step, turn) for step, turn in ORDER if turn < 2 // each]
+        at, turn = steps[0]
+        for i, (step_i, turn_i) in enumerate(steps[1:]):
+            at = jnp.where(k == i + 1, step_i, at)
+            turn = jnp.where(k == i + 1, turn_i, turn)
+        pair = chip + 1 - 2 * lax.rem(chip, 2)
+        there = jnp.where(
+            at == 0, chip, jnp.where(at == 1, pair, jnp.where(at == 2, lax.rem(chip + 2, 4), 3 - chip))
+        )
+        if each == 2:
+            return there
+        return 2 * there + lax.rem(side + turn, 2)
 
     def slot_rows(e):
         return pl.ds(pl.multiple_of(e * cap, cap), cap)
@@ -302,6 +346,18 @@
 
         lax.fori_loop(0, chunks, one, 0)
 
+    lead = 3
+    if groups == 8:
+        lead = jnp.where((g >= 2) & (g < 6), 3, 2)
+
+    def send_chunk(c):
+        for p in range(each):
+            target = c * each + p
+
+            @pl.when(target != g)
+            def _():
+                dispatch(target).start()
+
     def pack(k, carry_):
         c = chunk_of(k)
         at = pl.ds(pl.multiple_of(c * tall, tall), tall)
@@ -311,16 +367,16 @@
         def _():
             rows[own, mine] = packed[own, :]
 
-        for p in range(each):
-            target = c * each + p
-
-            @pl.when(target != g)
-            def _():
-                dispatch(target).start()
+        @pl.when(k <= lead)
+        def _():
+            send_chunk(c)
+
+        @pl.when(k == 0)
+        def _():
+            start_spread(c)
 
         return carry_
 
-    lax.fori_loop(0, chunks, pack, 0)
 
     def row_of(c):
         return pl.multiple_of(c * tall, tall)
@@ -362,49 +418,80 @@
         for copy in spread_relay(teams, j, hidden, row, tall, hide, c, h_send, h_recv):
             copy.start()
 
-    start_spread(chunk_of(0))
-    for load in loads[1:]:
+    lax.fori_loop(0, chunks, pack, 0)
+    for copy in square_copies():
+        copy.wait_recv()
+    total = ssq[0]
+    for p in range(1, teams):
+        total = total + ssq[p]
+    scale = lax.rsqrt(total * (1.0 / model) + EPSILON)
+    slot_scale = nt(scale, chooser[...].astype(f32), HIGHEST)
+    for e in range(groups):
+        scales[e, :, 0:cap] = slot_scale[:, e * cap : (e + 1) * cap]
+    scales_in[g] = scales[g]
+
+    def scale_copy(target):
+        return remote(scales.at[target], scales_in.at[g], n_send.at[target], n_recv.at[g], {"sp": target})
+
+    over_others(lambda target: scale_copy(target).start())
+    for load in loads[14:]:
         load.wait()
 
     def stage(k, carry_):
-        c = chunk_of(k)
-        last = chunk_of(jnp.maximum(k - 1, 0))
-        row = row_of(c)
+        @pl.when((k >= 1) & (k + lead < chunks))
+        def _():
+            send_chunk(chunk_of(k + lead))
+
+        @pl.when(k < chunks - 1)
+        def _():
+            start_spread(chunk_of(k + 1))
 
         @pl.when(k < chunks)
         def _():
+            c = chunk_of(k)
+            row = row_of(c)
             for copy in spread_own(teams, j, rows, row, tall, width, c, t_send, t_recv):
                 copy.wait_recv()
             for copy in spread_relay(teams, j, rows, row, tall, width, c, t_send, t_recv):
                 copy.start()
 
-        @pl.when(k < chunks - 1)
-        def _():
-            start_spread(chunk_of(k + 1))
-
-        @pl.when(k >= 1)
-        def _():
-            hidden_relay(last)
-
-        @pl.when(k < chunks)
-        def _():
+        @pl.when((k >= 1) & (k < chunks + 1))
+        def _():
+            c = chunk_of(k - 1)
+            row = row_of(c)
             for copy in spread_relay(teams, j, rows, row, tall, width, c, t_send, t_recv):
                 copy.wait_recv()
+            columns_ = []
+            for p in range(each):
+                source = c * each + p
+
+                @pl.when(source != g)
+                def _():
+                    place = scales_in.at[source]
+                    remote(place, place, n_send.at[source], n_recv.at[source], {"sp": source}).wait_recv()
+
+                line = scales_in[source][0:1, :]
+                columns_.append(jnp.broadcast_to(line, (128, 128)).T[0:cap, 0:1])
+            factor = columns_[0] if each == 1 else jnp.concatenate(columns_, axis=0)
             block_rows = rows[pl.ds(row, tall), :]
-            opened = jnp.dot(block_rows, gate[...], preferred_element_type=f32)
-            raised = jnp.dot(block_rows, up[...], preferred_element_type=f32)
+            opened = jnp.dot(block_rows, gate[...], preferred_element_type=f32) * factor
+            raised = jnp.dot(block_rows, up[...], preferred_element_type=f32) * factor
             made = (opened * jax.nn.sigmoid(opened) * raised).astype(bf16)
             hidden[pl.ds(row, tall), pl.ds(pl.multiple_of(j * hide, 128), hide)] = made
             for copy in spread_own(teams, j, hidden, row, tall, hide, c, h_send, h_recv):
                 copy.start()
 
-        @pl.when(k >= 1)
-        def _():
-            finish(last)
+        @pl.when((k >= 2) & (k < chunks + 2))
+        def _():
+            hidden_relay(chunk_of(k - 2))
+
+        @pl.when(k >= 3)
+        def _():
+            finish(chunk_of(k - 3))
 
         return carry_
 
-    lax.fori_loop(0, chunks + 1, stage, 0)
+    lax.fori_loop(0, chunks + 3, stage, 0)
 
     def await_back(source):
         place = returned.at[slot_rows(source)]
@@ -419,8 +506,19 @@
         @pl.when(g + r < groups)
         def _(r=r):
             send_table(r).wait_send()
+
+        @pl.when(sends(r))
+        def _(r=r):
             for h in range(heads):
                 for copy in send_pair(r, h):
+                    copy.wait_send()
+
+    if shared:
+
+        @pl.when(hands_on)
+        def _():
+            for h in range(heads):
+                for copy in hand_on(h):
                     copy.wait_send()
 
     for h in range(heads):
@@ -428,6 +526,7 @@
             copy.wait_send()
     for copy in square_copies():
         copy.wait_send()
+    over_others(lambda target: scale_copy(target).wait_send())
     over_others(lambda target: dispatch(target).wait_send())
     over_others(lambda target: give_back(target).wait_send())
 
@@ -441,10 +540,6 @@
         return carry_
 
     lax.fori_loop(0, chunks, drain, 0)
-
-
-def padded(a):
-    return jnp.pad(a, ((0, SUB - a.shape[0]), (0, 0)))
 
 
 def per_device(
@@ -480,25 +575,43 @@
     reach = max(1, groups // 4)
     ways = max(4, teams)
     others = teams - 1
-    decay = jax.nn.log_sigmoid(forget_gate_logits) + extra_log_decay
-    misc = jnp.concatenate(
-        [documents.astype(f32)[None, :], expert_choice_index.astype(f32).T, routing_weight.T], axis=0
+    arrays = (
+        cell_key_heads,
+        cell_value_heads,
+        forget_gate_logits.T,
+        input_gate_log.T,
+        extra_log_decay.T,
+        documents[None, :],
+        expert_choice_index.T,
+        routing_weight.T,
+        cell_query_heads,
+        output_gate_logits,
+        head_norm_gain[None, :],
+        stream,
+        expert_norm_gain,
+        output_weight,
+        gate_weight,
+        up_weight,
+        down_weight,
     )
-    table = jnp.concatenate([padded(decay.T), padded(input_gate_log.T), padded(misc)], axis=0)
     vmem = pl.BlockSpec(memory_space=pltpu.VMEM)
     hbm = pl.BlockSpec(memory_space=pl.ANY)
     dma = pltpu.SemaphoreType.DMA
     return pl.pallas_call(
         functools.partial(kernel, groups, teams, heads, reach, cap, each, chunks),
         out_shape=jax.ShapeDtypeStruct((tokens, width), bf16),
-        in_specs=[vmem] * 8 + [hbm] * 4,
+        in_specs=[hbm] * 17,
         out_specs=vmem,
         scratch_shapes=[
+            *(pltpu.VMEM(a.shape[-2:], a.dtype) for a in arrays),
+            pltpu.VMEM((3 * SUB, tokens), f32),
             pltpu.VMEM((reach, tokens, span), bf16),
             pltpu.VMEM((reach, tokens, span), bf16),
             pltpu.VMEM((reach, 3 * SUB, tokens), f32),
             pltpu.VMEM((tokens, teams * span), bf16),
             pltpu.VMEM((teams, SUB, tokens), f32),
+            pltpu.VMEM((groups, SUB, 128), f32),
+            pltpu.VMEM((groups, SUB, 128), f32),
             pltpu.VMEM((slots, tokens), bf16),
             pltpu.VMEM((tokens, slots), bf16),
             pltpu.VMEM((tokens, width), bf16),
@@ -508,21 +621,20 @@
             pltpu.VMEM((slots, hidden_all), bf16),
             pltpu.VMEM((slots, width), bf16),
             pltpu.VMEM((slots, width), bf16),
-            pltpu.VMEM(output_weight.shape, bf16),
-            pltpu.VMEM((model, hide), bf16),
-            pltpu.VMEM((model, hide), bf16),
-            pltpu.VMEM((hidden_all, width), bf16),
-            dma((4,)),
+            dma((len(arrays),)),
             dma((reach, heads)),
             dma((reach, heads)),
             dma((reach, heads)),
             dma((reach, heads)),
+            dma((2, heads)),
             dma((reach,)),
             dma((reach,)),
             dma((heads, others)),
             dma((heads, others)),
             dma((others,)),
             dma((others,)),
+            dma((groups,)),
+            dma((groups,)),
             dma((groups,)),
             dma((groups,)),
             dma((chunks, ways)),
@@ -535,20 +647,7 @@
         compiler_params=pltpu.CompilerParams(
             collective_id=1, has_side_effects=True, vmem_limit_bytes=VMEM_LIMIT
         ),
-    )(
-        cell_query_heads,
-        cell_key_heads,
-        cell_value_heads,
-        output_gate_logits,
-        table,
-        head_norm_gain[None, :],
-        stream,
-        expert_norm_gain[None, :],
-        output_weight,
-        gate_weight,
-        up_weight,
-        down_weight,
-    )
+    )(*arrays)
 
 
 def solution(mesh):

time: 105 us -> 87.3 us (0.83)
  Pallas kernels: 97.2 us -> 85.2 us
  other arithmetic: 4.03 us -> 0 us
  local copies, waits for them, and re-layouts: 2.94 us -> 1.67 us
    pallas_call x1, Pallas kernels: 97.2 us -> 85.2 us  [per_device(): pl.pallas_call(functools.partial(kernel, groups, teams, heads, reach, cap...]
    concatenate x2 -> x0, other arithmetic: 1.98 us -> none  [the longest x1 1.28 us: per_device(): jnp.concatenate([padded(decay.T), padded(input_gate_log.T), padded(misc)]...]
    transpose x2 -> x0, other arithmetic: 1.39 us -> none  [the longest x1 0.71 us: per_device(): table = jnp.concatenate([padded(decay.T), padded(input_gate_log.T), padde...]
    broadcast_in_dim x1 -> x0, local copies, waits for them, and re-layouts: 1.27 us -> none  [per_device(): expert_norm_gain[None, :]]
where the time goes in v2:
time: 87.3 us; the launch traced here: 86.9 us
  Pallas kernels  85.2 us (98%)
  local copies, waits for them, and re-layouts  1.67 us (2%)
    pallas_call x1, Pallas kernels, per_device(): pl.pallas_call(functools.partial(kernel, groups, teams, heads, reach, cap...  85.2 us

profile of v2, /device:TPU:9, one launch (start us, length us, event | category | flops | bytes accessed | tf_op | source)
XLA Modules:
  0.0 86.9 jit_solution(9082933675983793737)
XLA Ops:
  0.0 85.2 %shard_map.163 = bf16[128,1024]{1,0:T(8,128)(2,1)} custom-call(bf16[128,512]{1,0:T(8,128)(2,1)} %refs_0_.1, bf16[128,512]{1,0:T(8,128)(2,1)} %refs_1_.1, f32[4,128]{1,0:T(4,128)} %bitcast.7, f32[4,128]{1,0:T(4,128)} %bitcast.8, f32[4,128]{1,0:T(4,128)} %bitcast.9, s32[1,128]{1,0:T(1,128)} %bitcast.13, s32[2,128]{1,0:T(2,128)} %bitcast.11, ...), custom_call_target="tpu_custom_call" | custom-call | tf_op jit(solution)/shard_map/pallas_call | solution.py:600
  85.2 1.7 %copy.19 = bf16[128,1024]{1,0:T(8,128)(2,1)} copy(bf16[128,1024]{1,0:T(8,128)(2,1)} %shard_map.163) | data formatting | bytes 524288

commit v3 on v2

--- a/solution.py
+++ b/solution.py
@@ -16,7 +16,9 @@
 VMEM_LIMIT = 60 * 1024 * 1024
 SUB = 8
 EACH = 1
-ORDER = ((0, 0), (1, 0), (2, 0), (2, 1), (3, 0), (3, 1), (1, 1), (0, 1))
+PACES = ((-1, -1), (-1, -1), (-1, -1), (-1, -1), (1, 1), (2, 2), (3, 3), (4, 4))
+ORDER_MIDDLE = ((0, 0), (1, 0), (2, 0), (2, 1), (3, 0), (3, 1), (1, 1), (0, 1))
+ORDER_END = ((0, 0), (0, 1), (2, 0), (1, 0), (2, 1), (3, 0), (3, 1), (1, 1))
 f32, bf16 = jnp.float32, jnp.bfloat16
 
 
@@ -39,8 +41,7 @@
 def spread_own(teams, j, buf, row, height, width, chunk, send, recv):
     view = buf.at[pl.ds(row, height), pl.ds(pl.multiple_of(j * width, 128), width)]
     return [
-        remote(view, view, send.at[chunk, turn], recv.at[chunk, turn], {"tp": peer})
-        for turn, peer in enumerate(near_peers(teams, j))
+        remote(view, view, send.at[0], recv.at[chunk, 0], {"tp": peer}) for peer in near_peers(teams, j)
     ]
 
 
@@ -52,9 +53,27 @@
     first = buf.at[pl.ds(row, half), pl.ds(pl.multiple_of(across * width, 128), width)]
     second = buf.at[pl.ds(row + half, half), pl.ds(pl.multiple_of(along * width, 128), width)]
     return [
-        remote(first, first, send.at[chunk, 2], recv.at[chunk, 2], {"tp": along}),
-        remote(second, second, send.at[chunk, 3], recv.at[chunk, 3], {"tp": across}),
+        remote(first, first, send.at[0], recv.at[chunk, 1], {"tp": along}),
+        remote(second, second, send.at[0], recv.at[chunk, 1], {"tp": across}),
     ]
+
+
+def arrived(view, sem, g):
+    remote(view, view, sem, sem, {"sp": g}).wait_recv()
+
+
+def departed(view, sem, g):
+    remote(view, view, sem, sem, {"sp": g}).wait_send()
+
+
+def own_arrived(teams, g, buf, row, height, width, chunk, recv):
+    count = 2 if teams == 4 else teams - 1
+    arrived(buf.at[pl.ds(row, height), 0 : count * width], recv.at[chunk, 0], g)
+
+
+def relay_arrived(teams, g, buf, row, height, width, chunk, recv):
+    if teams == 4:
+        arrived(buf.at[pl.ds(row, height // 2), 0 : 2 * width], recv.at[chunk, 1], g)
 
 
 def nt(a, b, precision=None):
@@ -74,12 +93,13 @@
         wo, gate, up, down,
     ) = locals_
     (
-        table, kbuf, vbuf, tbuf, cell, ssq, scales, scales_in, chooser, comb, resid, normed, packed, rows, hidden,
+        table, kvbuf, tbuf, cell, ssq, scales, scales_in, chooser, comb, resid, normed, packed, rows, hidden,
         result, returned,
-        load_sem, k_send, k_recv, v_send, v_recv, f_send, m_send, m_recv, c_send, c_recv, s_send, s_recv,
-        n_send, n_recv, z_send, z_recv, t_send, t_recv, h_send, h_recv, r_send, r_recv,
+        load_sem, k_send, k_recv, f_send, m_send, m_recv, c_send, c_recv, s_send, s_recv,
+        o_sem, n_send, n_recv, z_send, z_recv, t_send, t_recv, h_send, h_recv, r_send, r_recv,
     ) = refs
     g, j = lax.axis_index("sp"), lax.axis_index("tp")
+    other = lax.rem(g + 1, groups)
     tokens, width = stream.shape
     hide = gate.shape[1]
     span = heads * HD
@@ -121,8 +141,8 @@
     def send_pair(r, h):
         cols = pl.ds(h * HD, HD)
         return [
-            remote(key.at[:, cols], kbuf.at[r - 1, :, cols], k_send.at[r - 1, h], k_recv.at[r - 1, h], {"sp": g + r}),
-            remote(value.at[:, cols], vbuf.at[r - 1, :, cols], v_send.at[r - 1, h], v_recv.at[r - 1, h], {"sp": g + r}),
+            remote(key.at[:, cols], kvbuf.at[r - 1, 0, :, cols], k_send.at[r - 1], k_recv.at[r - 1, h], {"sp": g + r}),
+            remote(value.at[:, cols], kvbuf.at[r - 1, 1, :, cols], k_send.at[r - 1], k_recv.at[r - 1, h], {"sp": g + r}),
         ]
 
     for r in range(1, reach + 1):
@@ -140,10 +160,8 @@
 
     def hand_on(h):
         cols = pl.ds(h * HD, HD)
-        return [
-            remote(kbuf.at[0, :, cols], kbuf.at[1, :, cols], f_send.at[0, h], k_recv.at[1, h], {"sp": g + 1}),
-            remote(vbuf.at[0, :, cols], vbuf.at[1, :, cols], f_send.at[1, h], v_recv.at[1, h], {"sp": g + 1}),
-        ]
+        view = kvbuf.at[0, :, :, cols]
+        return [remote(view, kvbuf.at[1, :, :, cols], f_send.at[0], k_recv.at[1, h], {"sp": g + 1})]
 
     for h in range(heads):
         for r in range(1, reach + 1):
@@ -157,8 +175,7 @@
 
         @pl.when(g < r)
         def _(r=r):
-            kbuf[r - 1] = jnp.zeros_like(kbuf[r - 1])
-            vbuf[r - 1] = jnp.zeros_like(vbuf[r - 1])
+            kvbuf[r - 1] = jnp.zeros_like(kvbuf[r - 1])
             tbuf[r - 1] = jnp.full(tbuf.shape[1:], -1.0, f32)
 
     down_iota = lax.broadcasted_iota(jnp.int32, (tokens, tokens), 0)
@@ -228,11 +245,12 @@
     for load in loads[8:13]:
         load.wait()
 
+    half = max(1, heads // 2)
+
     def cell_copies(h):
         view = cell.at[:, pl.ds(pl.multiple_of(j * span + h * HD, 128), HD)]
         return [
-            remote(view, view, c_send.at[h, turn], c_recv.at[h, turn], {"tp": peer})
-            for turn, peer in enumerate(peers)
+            remote(view, view, c_send.at[0], c_recv.at[h // half], {"tp": peer}) for peer in peers
         ]
 
     for h in range(heads):
@@ -241,8 +259,7 @@
 
             @pl.when(g >= r)
             def _(r=r, h=h):
-                for copy in send_pair(r, h):
-                    copy.wait_recv()
+                arrived(kvbuf.at[r - 1, :, :, pl.ds(h * HD, HD)], k_recv.at[r - 1, h], g - r)
 
             if shared and r == 1:
 
@@ -252,8 +269,8 @@
                         copy.start()
 
         q_h = query[:, cols]
-        keys = [key[:, cols]] + [kbuf[r, :, cols] for r in range(reach)]
-        values = [value[:, cols]] + [vbuf[r, :, cols] for r in range(reach)]
+        keys = [key[:, cols]] + [kvbuf[r, 0, :, cols] for r in range(reach)]
+        values = [value[:, cols]] + [kvbuf[r, 1, :, cols] for r in range(reach)]
         peak = carry[:, h : h + 1]
         logs = []
         for mask, term in zip(masks, terms):
@@ -275,12 +292,9 @@
             copy.start()
 
     loads[13].wait()
-    half = max(1, heads // 2)
     projected = stream[...].astype(f32)
     for first in range(0, heads, half):
-        for h in range(first, first + half):
-            for copy in cell_copies(h):
-                copy.wait_recv()
+        arrived(cell.at[:, 0 : half * HD * (teams - 1)], c_recv.at[first // half], other)
         for p in range(teams):
             piece = slice(p * span + first * HD, p * span + (first + half) * HD)
             projected = projected + jnp.dot(cell[:, piece], wo[piece, :], preferred_element_type=f32)
@@ -291,8 +305,7 @@
 
     def square_copies():
         return [
-            remote(ssq.at[j], ssq.at[j], s_send.at[turn], s_recv.at[turn], {"tp": peer})
-            for turn, peer in enumerate(peers)
+            remote(ssq.at[j], ssq.at[j], s_send.at[0], s_recv.at[0], {"tp": peer}) for peer in peers
         ]
 
     for copy in square_copies():
@@ -306,11 +319,17 @@
         if groups != 8:
             return lax.rem(block + k, chunks)
         chip, side = g // 2, lax.rem(g, 2)
-        steps = [(step, turn) for step, turn in ORDER if turn < 2 // each]
-        at, turn = steps[0]
-        for i, (step_i, turn_i) in enumerate(steps[1:]):
-            at = jnp.where(k == i + 1, step_i, at)
-            turn = jnp.where(k == i + 1, turn_i, turn)
+        middle = (g >= 2) & (g < 6)
+
+        def picked(order):
+            steps = [(step, turn) for step, turn in order if turn < 2 // each]
+            at, turn = steps[0]
+            for i, (step_i, turn_i) in enumerate(steps[1:]):
+                at = jnp.where(k == i + 1, step_i, at)
+                turn = jnp.where(k == i + 1, turn_i, turn)
+            return at, turn
+
+        at, turn = [jnp.where(middle, mid, end) for mid, end in zip(picked(ORDER_MIDDLE), picked(ORDER_END))]
         pair = chip + 1 - 2 * lax.rem(chip, 2)
         there = jnp.where(
             at == 0, chip, jnp.where(at == 1, pair, jnp.where(at == 2, lax.rem(chip + 2, 4), 3 - chip))
@@ -324,12 +343,12 @@
 
     def dispatch(target):
         return remote(
-            packed.at[slot_rows(target)], rows.at[own, mine], z_send.at[target], z_recv.at[g], {"sp": target}
+            packed.at[slot_rows(target)], rows.at[own, mine], z_send.at[0], z_recv.at[g], {"sp": target}
         )
 
     def give_back(target):
         return remote(
-            result.at[slot_rows(target)], returned.at[own], r_send.at[target], r_recv.at[g], {"sp": target}
+            result.at[slot_rows(target)], returned.at[own], r_send.at[0], r_recv.at[0], {"sp": target}
         )
 
     def over_others(body):
@@ -346,9 +365,19 @@
 
         lax.fori_loop(0, chunks, one, 0)
 
-    lead = 3
-    if groups == 8:
-        lead = jnp.where((g >= 2) & (g < 6), 3, 2)
+    lined = groups == 8 and each == 1
+    if lined:
+        middle = (g >= 2) & (g < 6)
+        paces = [jnp.where(middle, mid, end) for mid, end in PACES]
+    else:
+        paces = [max(-1, k - 3) for k in range(chunks)]
+
+    def issue(now):
+        for k, pace in enumerate(paces):
+
+            @pl.when(pace == now)
+            def _(k=k):
+                send_chunk(chunk_of(k))
 
     def send_chunk(c):
         for p in range(each):
@@ -367,9 +396,11 @@
         def _():
             rows[own, mine] = packed[own, :]
 
-        @pl.when(k <= lead)
-        def _():
-            send_chunk(c)
+        for i, pace in enumerate(paces):
+
+            @pl.when((k == i) & (pace == -1))
+            def _():
+                send_chunk(c)
 
         @pl.when(k == 0)
         def _():
@@ -388,15 +419,14 @@
             @pl.when(source != g)
             def _():
                 place = rows.at[slot_rows(source), mine]
-                remote(place, place, z_send.at[source], z_recv.at[source], {"sp": source}).wait_recv()
+                arrived(place, z_recv.at[source], source)
 
         for copy in spread_own(teams, j, rows, row_of(c), tall, width, c, t_send, t_recv):
             copy.start()
 
     def finish(c):
         row = row_of(c)
-        for copy in spread_relay(teams, j, hidden, row, tall, hide, c, h_send, h_recv):
-            copy.wait_recv()
+        relay_arrived(teams, other, hidden, row, tall, hide, c, h_recv)
         result[pl.ds(row, tall), :] = jnp.dot(
             hidden[pl.ds(row, tall), :], down[...], preferred_element_type=f32
         ).astype(bf16)
@@ -413,14 +443,12 @@
 
     def hidden_relay(c):
         row = row_of(c)
-        for copy in spread_own(teams, j, hidden, row, tall, hide, c, h_send, h_recv):
-            copy.wait_recv()
+        own_arrived(teams, other, hidden, row, tall, hide, c, h_recv)
         for copy in spread_relay(teams, j, hidden, row, tall, hide, c, h_send, h_recv):
             copy.start()
 
     lax.fori_loop(0, chunks, pack, 0)
-    for copy in square_copies():
-        copy.wait_recv()
+    arrived(ssq.at[0 : teams - 1], s_recv.at[0], other)
     total = ssq[0]
     for p in range(1, teams):
         total = total + ssq[p]
@@ -431,16 +459,14 @@
     scales_in[g] = scales[g]
 
     def scale_copy(target):
-        return remote(scales.at[target], scales_in.at[g], n_send.at[target], n_recv.at[g], {"sp": target})
+        return remote(scales.at[target], scales_in.at[g], n_send.at[0], n_recv.at[g], {"sp": target})
 
     over_others(lambda target: scale_copy(target).start())
     for load in loads[14:]:
         load.wait()
 
     def stage(k, carry_):
-        @pl.when((k >= 1) & (k + lead < chunks))
-        def _():
-            send_chunk(chunk_of(k + lead))
+        issue(k)
 
         @pl.when(k < chunks - 1)
         def _():
@@ -450,8 +476,7 @@
         def _():
             c = chunk_of(k)
             row = row_of(c)
-            for copy in spread_own(teams, j, rows, row, tall, width, c, t_send, t_recv):
-                copy.wait_recv()
+            own_arrived(teams, other, rows, row, tall, width, c, t_recv)
             for copy in spread_relay(teams, j, rows, row, tall, width, c, t_send, t_recv):
                 copy.start()
 
@@ -459,8 +484,7 @@
         def _():
             c = chunk_of(k - 1)
             row = row_of(c)
-            for copy in spread_relay(teams, j, rows, row, tall, width, c, t_send, t_recv):
-                copy.wait_recv()
+            relay_arrived(teams, other, rows, row, tall, width, c, t_recv)
             columns_ = []
             for p in range(each):
                 source = c * each + p
@@ -468,7 +492,7 @@
                 @pl.when(source != g)
                 def _():
                     place = scales_in.at[source]
-                    remote(place, place, n_send.at[source], n_recv.at[source], {"sp": source}).wait_recv()
+                    arrived(place, n_recv.at[source], source)
 
                 line = scales_in[source][0:1, :]
                 columns_.append(jnp.broadcast_to(line, (128, 128)).T[0:cap, 0:1])
@@ -493,14 +517,6 @@
 
     lax.fori_loop(0, chunks + 3, stage, 0)
 
-    def await_back(source):
-        place = returned.at[slot_rows(source)]
-        remote(place, place, r_send.at[source], r_recv.at[source], {"sp": source}).wait_recv()
-
-    over_others(await_back)
-    mixed = jnp.dot(comb[...], returned[...], preferred_element_type=f32)
-    out[...] = (resid[...].astype(f32) + mixed).astype(bf16)
-
     for r in range(1, reach + 1):
 
         @pl.when(g + r < groups)
@@ -509,37 +525,32 @@
 
         @pl.when(sends(r))
         def _(r=r):
-            for h in range(heads):
-                for copy in send_pair(r, h):
-                    copy.wait_send()
+            departed(kvbuf.at[r - 1], k_send.at[r - 1], g + r)
 
     if shared:
 
         @pl.when(hands_on)
         def _():
-            for h in range(heads):
-                for copy in hand_on(h):
-                    copy.wait_send()
-
-    for h in range(heads):
-        for copy in cell_copies(h):
-            copy.wait_send()
-    for copy in square_copies():
-        copy.wait_send()
-    over_others(lambda target: scale_copy(target).wait_send())
-    over_others(lambda target: dispatch(target).wait_send())
-    over_others(lambda target: give_back(target).wait_send())
-
-    def drain(c, carry_):
-        row = row_of(c)
-        for spread in (spread_own, spread_relay):
-            for copy in spread(teams, j, rows, row, tall, width, c, t_send, t_recv):
-                copy.wait_send()
-            for copy in spread(teams, j, hidden, row, tall, hide, c, h_send, h_recv):
-                copy.wait_send()
-        return carry_
-
-    lax.fori_loop(0, chunks, drain, 0)
+            departed(kvbuf.at[0], f_send.at[0], g + 1)
+
+    departed(cell.at[:, 0 : span * (teams - 1)], c_send.at[0], other)
+    departed(ssq.at[0 : teams - 1], s_send.at[0], other)
+    departed(scales.at[0 : groups - 1], n_send.at[0], other)
+    departed(packed.at[0 : (groups - 1) * cap], z_send.at[0], other)
+    departed(rows.at[:, 0 : (teams - 1) * width], t_send.at[0], other)
+    departed(hidden.at[:, 0 : (teams - 1) * hide], h_send.at[0], other)
+    arrived(returned.at[0 : (groups - 1) * cap], r_recv.at[0], other)
+    part = width // 2 if width % 256 == 0 else width
+    stores = []
+    for i in range(width // part):
+        cut = slice(i * part, (i + 1) * part)
+        mixed = jnp.dot(comb[...], returned[:, cut], preferred_element_type=f32)
+        resid[:, cut] = (resid[:, cut].astype(f32) + mixed).astype(bf16)
+        stores.append(pltpu.make_async_copy(resid.at[:, cut], out.at[:, cut], o_sem.at[i]))
+        stores[-1].start()
+    departed(result.at[0 : (groups - 1) * cap], r_send.at[0], other)
+    for store in stores:
+        store.wait()
 
 
 def per_device(
@@ -573,8 +584,6 @@
     each = max(1, min(groups, EACH * 64 // cap))
     chunks = groups // each
     reach = max(1, groups // 4)
-    ways = max(4, teams)
-    others = teams - 1
     arrays = (
         cell_key_heads,
         cell_value_heads,
@@ -594,19 +603,17 @@
         up_weight,
         down_weight,
     )
-    vmem = pl.BlockSpec(memory_space=pltpu.VMEM)
     hbm = pl.BlockSpec(memory_space=pl.ANY)
     dma = pltpu.SemaphoreType.DMA
     return pl.pallas_call(
         functools.partial(kernel, groups, teams, heads, reach, cap, each, chunks),
         out_shape=jax.ShapeDtypeStruct((tokens, width), bf16),
         in_specs=[hbm] * 17,
-        out_specs=vmem,
+        out_specs=hbm,
         scratch_shapes=[
             *(pltpu.VMEM(a.shape[-2:], a.dtype) for a in arrays),
             pltpu.VMEM((3 * SUB, tokens), f32),
-            pltpu.VMEM((reach, tokens, span), bf16),
-            pltpu.VMEM((reach, tokens, span), bf16),
+            pltpu.VMEM((reach, 2, tokens, span), bf16),
             pltpu.VMEM((reach, 3 * SUB, tokens), f32),
             pltpu.VMEM((tokens, teams * span), bf16),
             pltpu.VMEM((teams, SUB, tokens), f32),
@@ -622,27 +629,26 @@
             pltpu.VMEM((slots, width), bf16),
             pltpu.VMEM((slots, width), bf16),
             dma((len(arrays),)),
+            dma((reach,)),
             dma((reach, heads)),
-            dma((reach, heads)),
-            dma((reach, heads)),
-            dma((reach, heads)),
-            dma((2, heads)),
+            dma((1,)),
             dma((reach,)),
             dma((reach,)),
-            dma((heads, others)),
-            dma((heads, others)),
-            dma((others,)),
-            dma((others,)),
+            dma((1,)),
+            dma((2,)),
+            dma((1,)),
+            dma((1,)),
+            dma((2,)),
+            dma((1,)),
             dma((groups,)),
+            dma((1,)),
             dma((groups,)),
-            dma((groups,)),
-            dma((groups,)),
-            dma((chunks, ways)),
-            dma((chunks, ways)),
-            dma((chunks, ways)),
-            dma((chunks, ways)),
-            dma((groups,)),
-            dma((groups,)),
+            dma((1,)),
+            dma((chunks, 2)),
+            dma((1,)),
+            dma((chunks, 2)),
+            dma((1,)),
+            dma((1,)),
         ],
         compiler_params=pltpu.CompilerParams(
             collective_id=1, has_side_effects=True, vmem_limit_bytes=VMEM_LIMIT

time: 87.3 us -> 84.7 us (0.970)
  Pallas kernels: 85.2 us -> 82.7 us
    pallas_call x1, Pallas kernels: 85.2 us -> 82.7 us  [per_device(): pl.pallas_call(functools.partial(kernel, groups, teams, heads, reach, cap...]
where the time goes in v3:
time: 84.7 us; the launch traced here: 84.4 us
  Pallas kernels  82.7 us (98%)
  local copies, waits for them, and re-layouts  1.67 us (2%)
    pallas_call x1, Pallas kernels, per_device(): pl.pallas_call(functools.partial(kernel, groups, teams, heads, reach, cap...  82.7 us

profile of v3, /device:TPU:9, one launch (start us, length us, event | category | flops | bytes accessed | tf_op | source)
XLA Modules:
  0.0 84.4 jit_solution(12969658297158257487)
XLA Ops:
  0.0 82.7 %shard_map.163 = bf16[128,1024]{1,0:T(8,128)(2,1)} custom-call(bf16[128,512]{1,0:T(8,128)(2,1)} %refs_0_.1, bf16[128,512]{1,0:T(8,128)(2,1)} %refs_1_.1, f32[4,128]{1,0:T(4,128)} %bitcast.7, f32[4,128]{1,0:T(4,128)} %bitcast.8, f32[4,128]{1,0:T(4,128)} %bitcast.9, s32[1,128]{1,0:T(1,128)} %bitcast.13, s32[2,128]{1,0:T(2,128)} %bitcast.11, ...), custom_call_target="tpu_custom_call" | custom-call | tf_op jit(solution)/shard_map/pallas_call | solution.py:608
  82.7 1.7 %copy.19 = bf16[128,1024]{1,0:T(8,128)(2,1)} copy(bf16[128,1024]{1,0:T(8,128)(2,1)} %shard_map.163) | data formatting | bytes 524288

commit v4 on v3

--- a/solution.py
+++ b/solution.py
@@ -373,10 +373,11 @@
         paces = [max(-1, k - 3) for k in range(chunks)]
 
     def issue(now):
-        for k, pace in enumerate(paces):
+        for k, pace in list(enumerate(paces))[early:]:
 
             @pl.when(pace == now)
             def _(k=k):
+                pack_chunk(chunk_of(k))
                 send_chunk(chunk_of(k))
 
     def send_chunk(c):
@@ -387,27 +388,28 @@
             def _():
                 dispatch(target).start()
 
-    def pack(k, carry_):
-        c = chunk_of(k)
+    early = 4 if lined else min(chunks, 3)
+
+    def pack_chunk(c):
         at = pl.ds(pl.multiple_of(c * tall, tall), tall)
         packed[at, :] = jnp.dot(chooser[at, :], normed[...], preferred_element_type=f32).astype(bf16)
 
+    def pack(turn, carry_):
+        k = jnp.where(turn == 0, 2, jnp.where(turn <= 2, turn - 1, turn)) if lined else turn
+        c = chunk_of(k)
+        pack_chunk(c)
+
         @pl.when(k == 0)
         def _():
             rows[own, mine] = packed[own, :]
 
-        for i, pace in enumerate(paces):
-
-            @pl.when((k == i) & (pace == -1))
-            def _():
-                send_chunk(c)
+        send_chunk(c)
 
         @pl.when(k == 0)
         def _():
             start_spread(c)
 
         return carry_
-
 
     def row_of(c):
         return pl.multiple_of(c * tall, tall)
@@ -447,7 +449,7 @@
         for copy in spread_relay(teams, j, hidden, row, tall, hide, c, h_send, h_recv):
             copy.start()
 
-    lax.fori_loop(0, chunks, pack, 0)
+    lax.fori_loop(0, early, pack, 0)
     arrived(ssq.at[0 : teams - 1], s_recv.at[0], other)
     total = ssq[0]
     for p in range(1, teams):

time: 84.7 us -> 84.6 us (level)
  no operation moved by 1% of the time
where the time goes in v4:
time: 84.6 us; the launch traced here: 84.4 us
  Pallas kernels  82.7 us (98%)
  local copies, waits for them, and re-layouts  1.67 us (2%)
    pallas_call x1, Pallas kernels, per_device(): pl.pallas_call(functools.partial(kernel, groups, teams, heads, reach, cap...  82.7 us

profile of v4, /device:TPU:9, one launch (start us, length us, event | category | flops | bytes accessed | tf_op | source)
XLA Modules:
  0.0 84.4 jit_solution(10711761810373397418)
XLA Ops:
  0.0 82.7 %shard_map.163 = bf16[128,1024]{1,0:T(8,128)(2,1)} custom-call(bf16[128,512]{1,0:T(8,128)(2,1)} %refs_0_.1, bf16[128,512]{1,0:T(8,128)(2,1)} %refs_1_.1, f32[4,128]{1,0:T(4,128)} %bitcast.7, f32[4,128]{1,0:T(4,128)} %bitcast.8, f32[4,128]{1,0:T(4,128)} %bitcast.9, s32[1,128]{1,0:T(1,128)} %bitcast.13, s32[2,128]{1,0:T(2,128)} %bitcast.11, ...), custom_call_target="tpu_custom_call" | custom-call | tf_op jit(solution)/shard_map/pallas_call | solution.py:610
  82.7 1.7 %copy.19 = bf16[128,1024]{1,0:T(8,128)(2,1)} copy(bf16[128,1024]{1,0:T(8,128)(2,1)} %shard_map.163) | data formatting | bytes 524288
